TPU v7x, 768 devices: a whole 4x8x12 slice. The times are simulated.
768 devices in a mesh: ep: 48 (over z, x), tp: 16 (over y, core).
Axes of the slice: x: 4, y: 8, z: 12, core: 2. Of those that a mesh axis runs over, the one named last changes fastest.
Arguments:
- tokens: bfloat16 [336, 2304], P('ep'), may hold values from -6 to 6
- attn_gain: bfloat16 [2304], replicated, may hold values from 0.099609375 to 1.8984375
- query_weight: bfloat16 [2304, 2048], P(None, 'tp'), may hold values from -0.125 to 0.125
- key_weight: bfloat16 [2304, 2048], P(None, 'tp'), may hold values from -0.125 to 0.125
- value_weight: bfloat16 [2304, 2048], P(None, 'tp'), may hold values from -0.125 to 0.125
- out_weight: bfloat16 [2304, 2048], P(None, 'tp'), may hold values from -0.125 to 0.125
- lambdas: float32 [16], P('tp'), may hold values from 0.3 to 0.8
- head_gain: bfloat16 [128], replicated, may hold values from 0.099609375 to 1.8984375
- cache_keys: bfloat16 [336, 1024, 16, 128], P('ep', None, 'tp'), may hold values from -1500 to 1500
- cache_values: bfloat16 [336, 1024, 16, 128], P('ep', None, 'tp'), may hold values from -6 to 6
- lengths: int32 [336], P('ep'), may hold values from 2 to 1024, as said below
- moe_gain: bfloat16 [2304], replicated, may hold values from 0.099609375 to 1.8984375
- gate_weight: bfloat16 [48, 2304, 1024], P('ep', None, 'tp'), may hold values from -0.125 to 0.125
- up_weight: bfloat16 [48, 2304, 1024], P('ep', None, 'tp'), may hold values from -0.125 to 0.125
- down_weight: bfloat16 [48, 1024, 2304], P('ep', 'tp'), may hold values from -0.1875 to 0.1875
- shared_gate: bfloat16 [2304, 1024], P(None, 'tp'), may hold values from -0.125 to 0.125
- shared_up: bfloat16 [2304, 1024], P(None, 'tp'), may hold values from -0.125 to 0.125
- shared_down: bfloat16 [1024, 2304], P('tp'), may hold values from -0.1875 to 0.1875
- expert_ids: int32 [336, 6], P('ep'), may hold values from 0 to 47, all different within a row; in each aligned block of 7 rows (0 to 6, 7 to 13, ...) at most 2 rows name the same one
- expert_weights: float32 [336, 6], P('ep'), may hold values from 0.2 to 1
Outputs:
- result: bfloat16 [336, 2304], P('ep', 'tp')
Inputs may be any that keep to these rules, and one draw needn't show every extreme that they name: `expert_ids`: each row names 6 different experts. Among the rows of one device (aligned blocks of 7 rows) no expert is named by more than 2 rows, a bound that some block reaches. `lengths`: some sequence has 1024 cached positions.
All inputs are finite; a program needn't handle non-finite values.
Results may differ from a plain program's by a relative error of at most 0.02.
Values may be sent and summed in bfloat16 or wider, within the bound.
A program may use at most 32 MiB of HBM per device.

v0:
```python
import jax
import jax.numpy as jnp
from jax import lax
from jax.sharding import PartitionSpec as P

epsilon = 1e-06


def over_pieces(array, axis):
    return lax.all_gather(array, axis).astype(jnp.float32).sum(0)


def cut_along(array, dim, size):
    shape = array.shape
    parts = array.reshape(*shape[:dim], size, shape[dim] // size, *shape[dim + 1 :])
    return jnp.moveaxis(parts, dim, 0)


def sum_at_owner(array, axis, dim):
    size = lax.axis_size(axis)
    parts = lax.all_to_all(cut_along(array, dim, size), axis, 0, 0, tiled=True)
    return jnp.sum(parts.astype(jnp.float32), axis=0)


def sent_together(arrays, axis, dim, along):
    both = jnp.concatenate(arrays, axis=along)
    whole, at, gathered = (sum_at_owner(both, axis, dim), 0, [])
    for a in arrays:
        gathered.append(lax.slice_in_dim(whole, at, at + a.shape[along], axis=along))
        at += a.shape[along]
    return tuple(gathered)


def rms_scale(values, gain):
    wide = values.astype(jnp.float32)
    return (
        wide
        * lax.rsqrt(jnp.mean(wide * wide, axis=-1, keepdims=True) + epsilon)
        * gain.astype(jnp.float32)
    )


def shards(
    tokens,
    attn_gain,
    query_weight,
    key_weight,
    value_weight,
    out_weight,
    lambdas,
    head_gain,
    cache_keys,
    cache_values,
    lengths,
    moe_gain,
    gate_weight,
    up_weight,
    down_weight,
    shared_gate,
    shared_up,
    shared_down,
    expert_ids,
    expert_weights,
):
    seq_dev, model_width = tokens.shape
    local_heads = lambdas.shape[0]
    head_dim = cache_keys.shape[-1] // 2
    cache_len = cache_keys.shape[1]
    normed = rms_scale(tokens, attn_gain).astype(jnp.bfloat16)
    query_rows = jnp.dot(normed, query_weight, preferred_element_type=jnp.float32).astype(
        jnp.bfloat16
    )
    key_new = jnp.dot(normed, key_weight, preferred_element_type=jnp.float32).astype(jnp.bfloat16)
    value_new = jnp.dot(normed, value_weight, preferred_element_type=jnp.float32).astype(
        jnp.bfloat16
    )
    score_scale = head_dim ** (-0.5)
    queries = query_rows.reshape(seq_dev, local_heads, 2, head_dim)
    new_keys = key_new.reshape(seq_dev, local_heads, 2, head_dim)
    new_values = value_new.reshape(seq_dev, local_heads, 2 * head_dim)
    past_keys = cache_keys.reshape(seq_dev, cache_len, local_heads, 2, head_dim)
    scores = (
        jnp.einsum("shmd,sjhmd->shmj", queries, past_keys, preferred_element_type=jnp.float32)
        * score_scale
    )
    own_score = (
        jnp.sum(queries.astype(jnp.float32) * new_keys.astype(jnp.float32), axis=-1) * score_scale
    )
    live_mask = (jnp.arange(cache_len, dtype=jnp.int32)[None, :] < lengths[:, None])[
        :, None, None, :
    ]
    peak_score = jnp.maximum(jnp.max(jnp.where(live_mask, scores, -jnp.inf), axis=-1), own_score)
    exp_terms = jnp.where(live_mask, jnp.exp(scores - peak_score[..., None]), 0.0)
    own_term = jnp.exp(own_score - peak_score)
    denom_sum = jnp.sum(exp_terms, axis=-1) + own_term
    map_probs = exp_terms / denom_sum[..., None]
    own_prob = own_term / denom_sum
    lambda_row = lambdas[None, :]
    mixture = (map_probs[:, :, 0] - lambda_row[..., None] * map_probs[:, :, 1]).astype(jnp.bfloat16)
    own_mixture = (own_prob[:, :, 0] - lambda_row * own_prob[:, :, 1]).astype(jnp.bfloat16)
    head_out = jnp.einsum(
        "shj,sjhv->shv", mixture, cache_values, preferred_element_type=jnp.float32
    )
    head_out = head_out + own_mixture.astype(jnp.float32)[..., None] * new_values.astype(
        jnp.float32
    )
    head_normed = (
        rms_scale(head_out, head_gain)
        .astype(jnp.bfloat16)
        .reshape(seq_dev, local_heads * 2 * head_dim)
    )
    attn_part = lax.dot_general(
        head_normed, out_weight, (((1,), (1,)), ((), ())), preferred_element_type=jnp.float32
    )
    attn_total = over_pieces(attn_part.astype(jnp.bfloat16), "tp").astype(jnp.float32)
    mixed_rows = (tokens.astype(jnp.float32) + attn_total).astype(jnp.bfloat16)
    moe_normed = rms_scale(mixed_rows, moe_gain).astype(jnp.bfloat16)
    shared_gate_out = jnp.dot(moe_normed, shared_gate, preferred_element_type=jnp.float32)
    shared_up_out = jnp.dot(moe_normed, shared_up, preferred_element_type=jnp.float32)
    shared_hidden = (jax.nn.silu(shared_gate_out) * shared_up_out).astype(jnp.bfloat16)
    shared_part = jnp.dot(shared_hidden, shared_down, preferred_element_type=jnp.float32)
    experts = lax.axis_size("ep")
    top_count = expert_ids.shape[1]
    capacity = min(seq_dev, max(2, 2 * seq_dev * top_count // experts))
    slot_count = seq_dev * top_count
    slot_ids = expert_ids.reshape(slot_count)
    expert_hits = (slot_ids[:, None] == jnp.arange(experts, dtype=jnp.int32)[None, :]).astype(
        jnp.int32
    )
    slot_rank = jnp.sum((jnp.cumsum(expert_hits, axis=0) - expert_hits) * expert_hits, axis=1)
    slot_place = slot_ids * capacity + slot_rank
    placed = (
        slot_place[:, None] == jnp.arange(experts * capacity, dtype=jnp.int32)[None, :]
    ).astype(jnp.bfloat16)
    slot_token = jnp.arange(slot_count, dtype=jnp.int32) // top_count
    token_pick = (slot_token[:, None] == jnp.arange(seq_dev, dtype=jnp.int32)[None, :]).astype(
        jnp.bfloat16
    )
    dispatch = lax.dot_general(
        placed, token_pick, (((0,), (0,)), ((), ())), preferred_element_type=jnp.float32
    ).astype(jnp.bfloat16)
    col_count = model_width // lax.axis_size("tp")
    own_start = lax.axis_index("tp") * col_count
    send_rows = jnp.dot(dispatch, moe_normed, preferred_element_type=jnp.float32).astype(
        jnp.bfloat16
    )
    received = lax.all_to_all(send_rows, "ep", split_axis=0, concat_axis=0, tiled=True)
    gate_out = jnp.dot(received, gate_weight[0], preferred_element_type=jnp.float32)
    up_out = jnp.dot(received, up_weight[0], preferred_element_type=jnp.float32)
    expert_hidden = (jax.nn.silu(gate_out) * up_out).astype(jnp.bfloat16)
    expert_part = jnp.dot(expert_hidden, down_weight[0], preferred_element_type=jnp.float32)
    expert_sum, shared_out = sent_together(
        (expert_part.astype(jnp.bfloat16), shared_part.astype(jnp.bfloat16)), "tp", 1, 0
    )
    returned = lax.all_to_all(
        expert_sum.astype(jnp.bfloat16), "ep", split_axis=0, concat_axis=0, tiled=True
    )
    slot_values = jnp.dot(placed, returned, preferred_element_type=jnp.float32).reshape(
        seq_dev, top_count, col_count
    )
    routed = jnp.sum(expert_weights[:, :, None] * slot_values, axis=1)
    own_cols = lax.dynamic_slice_in_dim(mixed_rows, own_start, col_count, 1)
    return (own_cols.astype(jnp.float32) + routed + shared_out).astype(jnp.bfloat16)


def solution(mesh):
    in_specs = (
        P("ep", None),
        P(),
        P(None, "tp"),
        P(None, "tp"),
        P(None, "tp"),
        P(None, "tp"),
        P("tp"),
        P(),
        P("ep", None, "tp", None),
        P("ep", None, "tp", None),
        P("ep"),
        P(),
        P("ep", None, "tp"),
        P("ep", None, "tp"),
        P("ep", "tp", None),
        P(None, "tp"),
        P(None, "tp"),
        P("tp", None),
        P("ep", None),
        P("ep", None),
    )
    out_specs = P("ep", "tp")
    return jax.shard_map(shards, mesh=mesh, in_specs=in_specs, out_specs=out_specs, check_vma=False)
```

profile of v0, /device:TPU:1, one launch (start us, length us, event | category | flops | bytes accessed | tf_op | source)
XLA Modules:
  0.0 121.3 jit_solution(7295321418513757389)
XLA Ops:
  0.0 0.8 convert_element_type.125
  0.8 0.9 fusion.19
  1.7 1.3 %convolution_convert_fusion.6 = bf16[7,128]{1,0:T(8,128)(2,1)S(1)} fusion(bf16[2304,128]{1,0:T(8,128)(2,1)} %param.22, bf16[7,2304]{1,0:T(8,128)(2,1)} %param.20, f32[2304]{0:T(1024)S(1)} %convert_element_type.125, f32[7]{0:T(128)S(1)} %add_rsqrt_fusion.2), kind=kOutput, calls=%fused_computation.16 | convolution fusion | flops 4194176 | bytes 633116 | tf_op jit(solution)/shard_map/dot_general | solution.py:70
  3.2 3.9 %copy.44 = bf16[7,1024,1,128]{1,3,0,2:T(8,128)(2,1)} copy(bf16[7,1024,1,128]{3,1,2,0:T(8,128)(2,1)} %param.28) | data formatting | bytes 3670016 | tf_op args[8]
  7.2 0.2 fusion.7
  7.7 1.9 %fusion.63 = f32[7,2,1,1024]{3,2,1,0:T(1,128)S(1)} fusion(bf16[7,2,64,1]{2,3,1,0:T(2,128)(2,1)S(1)} %reshape.286, bf16[7,1024,2,64]{1,3,2,0:T(8,128)(2,1)} %bitcast.66), kind=kOutput, calls=%fused_computation.99 | convolution fusion | flops 1835008 | bytes 1894144 | tf_op jit(solution)/shard_map/shmd,sjhmd->shmj/dot_general | solution.py:83
  9.7 0.2 fusion.23
  10.7 0.3 fusion.1
  11.1 0.4 multiply_reduce_fusion
  11.5 0.3 fusion
  11.8 26.3 %all-gather.1 = bf16[16,7,2304]{2,1,0:T(8,128)(2,1)S(1)} all-gather(bf16[1,7,2304]{2,1,0:T(8,128)(2,1)S(1)} %fusion), channel_id=2, replica_groups=mesh['ep'=48,'tp'=16] {'tp'}, dimensions={0}, use_global_device_ids=true | all-gather | bytes 548352 | tf_op jit(solution)/shard_map/all_gather | solution.py:10
  38.1 0.1 convert_reduce_fusion
  38.2 0.1 fusion.16
  38.6 0.2 select_reduce_fusion.1
  38.8 0.6 convolution_convert_fusion.1
  39.4 0.9 all_to_all.19
  40.4 12.4 %all-to-all-start = ((bf16[48,2,2304]{2,1,0:T(2,128)(2,1)}), bf16[48,2,2304]{2,1,0:T(2,128)(2,1)S(1)}, u32[]{:S(2)}, u32[]{:S(2)}) async-start(bf16[48,2,2304]{2,1,0:T(2,128)(2,1)} %all_to_all.19), calls=%async_computation | async-start | bytes 884736 | tf_op jit(solution)/shard_map/all_to_all | solution.py:147
  52.8 1.2 fusion.59
  54.0 1.1 convolution_convert_fusion.2
  55.1 18.9 %all-to-all-done = bf16[48,2,2304]{2,1,0:T(2,128)(2,1)S(1)} async-done(((bf16[48,2,2304]{2,1,0:T(2,128)(2,1)}), bf16[48,2,2304]{2,1,0:T(2,128)(2,1)S(1)}, u32[]{:S(2)}, u32[]{:S(2)}) %all-to-all-start) | async-done | bytes 442400 | tf_op jit(solution)/shard_map/all_to_all | solution.py:147
  74.0 0.2 all_to_all.21
  74.2 0.3 fusion.14
  74.5 1.7 %convolution_convert_fusion = bf16[96,2304]{1,0:T(8,128)(2,1)S(1)} fusion(bf16[96,2304]{1,0:T(8,128)(2,1)S(1)} %all_to_all.21, bf16[1,64,2304]{2,1,0:T(8,128)(2,1)S(1)} %copy-done.7, bf16[1,2304,64]{1,2,0:T(8,128)(2,1)} %param.33, f32[96,64]{0,1:T(8,128)S(1)} %fusion.14), kind=kOutput, calls=%fused_computation | convolution fusion | flops 56881152 | bytes 1499136 | tf_op jit(solution)/shard_map/dot_general | solution.py:151
  76.3 1.1 copy.48
  77.4 7.3 %all-to-all-start.1 = ((bf16[16,103,144]{1,2,0:T(8,128)(2,1)}), bf16[16,103,144]{1,2,0:T(8,128)(2,1)S(1)}, u32[]{:S(2)}, u32[]{:S(2)}) async-start(bf16[16,103,144]{1,2,0:T(8,128)(2,1)} %bitcast.18), calls=%async_computation.1 | async-start | bytes 1179648 | tf_op jit(solution)/shard_map/all_to_all | solution.py:21
  84.8 18.5 %all-to-all-done.1 = bf16[16,103,144]{1,2,0:T(8,128)(2,1)S(1)} async-done(((bf16[16,103,144]{1,2,0:T(8,128)(2,1)}), bf16[16,103,144]{1,2,0:T(8,128)(2,1)S(1)}, u32[]{:S(2)}, u32[]{:S(2)}) %all-to-all-start.1) | async-done | bytes 474656 | tf_op jit(solution)/shard_map/all_to_all | solution.py:21
  103.2 0.1 convert_reduce_fusion.1
  103.5 0.7 all_to_all.23
  104.1 5.0 %all-to-all-start.2 = ((bf16[48,2,144]{2,1,0:T(2,128)(2,1)}), bf16[48,2,144]{2,1,0:T(2,128)(2,1)S(1)}, u32[]{:S(2)}, u32[]{:S(2)}) async-start(bf16[48,2,144]{2,1,0:T(2,128)(2,1)} %all_to_all.23), calls=%async_computation.2 | async-start | bytes 98304 | tf_op jit(solution)/shard_map/all_to_all | solution.py:155
  109.5 10.8 %all-to-all-done.2 = bf16[48,2,144]{2,1,0:T(2,128)(2,1)S(1)} async-done(((bf16[48,2,144]{2,1,0:T(2,128)(2,1)}), bf16[48,2,144]{2,1,0:T(2,128)(2,1)S(1)}, u32[]{:S(2)}, u32[]{:S(2)}) %all-to-all-start.2) | async-done | bytes 27680 | tf_op jit(solution)/shard_map/all_to_all | solution.py:155
  120.4 0.2 fusion.3
  120.6 0.7 add_convert_fusion
  (61 shorter events, 1.6 us)
Async XLA Ops:
  0.0 10.7 %copy-start = (bf16[7,1024,1,128]{3,1,2,0:T(8,128)(2,1)S(1)}, bf16[7,1024,1,128]{3,1,2,0:T(8,128)(2,1)}, u32[]{:S(2)}) copy-start(bf16[7,1024,1,128]{3,1,2,0:T(8,128)(2,1)} %param.29) | copy-start | bytes 5505028
  3.2 3.9 %copy-start.12 = (s32[7]{0:T(128)S(1)}, s32[7]{0:T(128)}, u32[]{:S(2)}) copy-start(s32[7]{0:T(128)} %param.30) | copy-start | bytes 88
  3.2 4.0 %copy-start.1 = (bf16[7,2304]{1,0:T(8,128)(2,1)S(1)}, bf16[7,2304]{1,0:T(8,128)(2,1)}, u32[]{:S(2)}) copy-start(bf16[7,2304]{1,0:T(8,128)(2,1)} %param.20) | copy-start | bytes 96772
  3.2 4.0 %copy-start.2 = (bf16[2304,128]{1,0:T(8,128)(2,1)S(1)}, bf16[2304,128]{1,0:T(8,128)(2,1)}, u32[]{:S(2)}) copy-start(bf16[2304,128]{1,0:T(8,128)(2,1)} %param.23) | copy-start | bytes 1769476
  7.7 3.4 %copy-start.13 = (bf16[2304,128]{1,0:T(8,128)(2,1)S(1)}, bf16[2304,128]{1,0:T(8,128)(2,1)}, u32[]{:S(2)}) copy-start(bf16[2304,128]{1,0:T(8,128)(2,1)} %param.24) | copy-start | bytes 1769476
  9.6 1.9 %copy-start.14 = (bf16[128]{0:T(256)(128)(2,1)S(1)}, bf16[128]{0:T(256)(128)(2,1)}, u32[]{:S(2)}) copy-start(bf16[128]{0:T(256)(128)(2,1)} %param.27) | copy-start | bytes 772
  9.6 1.9 %copy-start.3 = (bf16[2304,128]{1,0:T(8,128)(2,1)S(1)}, bf16[2304,128]{1,0:T(8,128)(2,1)}, u32[]{:S(2)}) copy-start(bf16[2304,128]{1,0:T(8,128)(2,1)} %param.25) | copy-start | bytes 1769476
  11.1 27.3 %copy-start.9 = (s32[7,6]{1,0:T(8,128)S(1)}, s32[7,6]{1,0:T(8,128)}, u32[]{:S(2)}) copy-start(s32[7,6]{1,0:T(8,128)} %param.38) | copy-start | bytes 508
  11.1 27.7 %copy-start.10 = (bf16[2304]{0:T(1024)(128)(2,1)S(1)}, bf16[2304]{0:T(1024)(128)(2,1)}, u32[]{:S(2)}) copy-start(bf16[2304]{0:T(1024)(128)(2,1)} %param.31) | copy-start | bytes 13828
  38.1 15.9 %copy-start.5 = (bf16[64,2304]{1,0:T(8,128)(2,1)S(1)}, bf16[64,2304]{1,0:T(8,128)(2,1)}, u32[]{:S(2)}) copy-start(bf16[64,2304]{1,0:T(8,128)(2,1)} %param.37) | copy-start | bytes 884740
  38.1 15.9 %copy-start.6 = (bf16[2304,64]{0,1:T(8,128)(2,1)S(1)}, bf16[2304,64]{0,1:T(8,128)(2,1)}, u32[]{:S(2)}) copy-start(bf16[2304,64]{0,1:T(8,128)(2,1)} %param.36) | copy-start | bytes 884740
  39.4 34.8 %copy-start.4 = (bf16[1,2304,64]{1,2,0:T(8,128)(2,1)S(1)}, bf16[1,2304,64]{1,2,0:T(8,128)(2,1)}, u32[]{:S(2)}) copy-start(bf16[1,2304,64]{1,2,0:T(8,128)(2,1)} %param.32) | copy-start | bytes 884740
  40.4 34.1 %copy-start.7 = (bf16[1,64,2304]{2,1,0:T(8,128)(2,1)S(1)}, bf16[1,64,2304]{2,1,0:T(8,128)(2,1)}, u32[]{:S(2)}) copy-start(bf16[1,64,2304]{2,1,0:T(8,128)(2,1)} %param.34) | copy-start | bytes 884740
  40.4 33.7 %all-to-all-start = ((bf16[48,2,2304]{2,1,0:T(2,128)(2,1)}), bf16[48,2,2304]{2,1,0:T(2,128)(2,1)S(1)}, u32[]{:S(2)}, u32[]{:S(2)}) async-start(bf16[48,2,2304]{2,1,0:T(2,128)(2,1)} %all_to_all.19), calls=%async_computation | async-start | bytes 884736 | tf_op jit(solution)/shard_map/all_to_all | solution.py:147
  74.2 2.0 %copy-start.8 = (bf16[7,2304]{1,0:T(8,128)(2,1)S(1)}, bf16[7,2304]{1,0:T(8,128)(2,1)}, u32[]{:S(2)}) copy-start(bf16[7,2304]{1,0:T(8,128)(2,1)} %convolution_convert_fusion.2) | copy-start | bytes 96772
  76.3 33.0 %copy-start.11 = (f32[7,6]{1,0:T(8,128)S(1)}, f32[7,6]{1,0:T(8,128)}, u32[]{:S(2)}) copy-start(f32[7,6]{1,0:T(8,128)} %param.39) | copy-start | bytes 508
  77.4 25.9 %all-to-all-start.1 = ((bf16[16,103,144]{1,2,0:T(8,128)(2,1)}), bf16[16,103,144]{1,2,0:T(8,128)(2,1)S(1)}, u32[]{:S(2)}, u32[]{:S(2)}) async-start(bf16[16,103,144]{1,2,0:T(8,128)(2,1)} %bitcast.18), calls=%async_computation.1 | async-start | bytes 1179648 | tf_op jit(solution)/shard_map/all_to_all | solution.py:21
  104.1 16.2 %all-to-all-start.2 = ((bf16[48,2,144]{2,1,0:T(2,128)(2,1)}), bf16[48,2,144]{2,1,0:T(2,128)(2,1)S(1)}, u32[]{:S(2)}, u32[]{:S(2)}) async-start(bf16[48,2,144]{2,1,0:T(2,128)(2,1)} %all_to_all.23), calls=%async_computation.2 | async-start | bytes 98304 | tf_op jit(solution)/shard_map/all_to_all | solution.py:155
where the time goes:
time: 122 us; the launch traced here: 121 us
  waiting for transfers between devices  48.2 us (40%)
  blocking collectives  26.3 us (22%)
  starting transfers between devices  24.7 us (20%)
  matrix products  9.57 us (8%)
  local copies, waits for them, and re-layouts  7.72 us (6%)
  other arithmetic  3.79 us (3%)
    all_gather x1, blocking collectives, over_pieces(): return lax.all_gather(array, axis).astype(jnp.float32).sum(0)  26.3 us
    all_to_all x1, waiting for transfers between devices, shards(): lax.all_to_all(send_rows, 'ep', split_axis=0, concat_axis=0, tiled=True)  18.9 us
    all_to_all x1, waiting for transfers between devices, sum_at_owner(): parts = lax.all_to_all(cut_along(array, dim, size), axis, 0, 0, tiled=True)  18.5 us
    all_to_all x1, starting transfers between devices, shards(): lax.all_to_all(send_rows, 'ep', split_axis=0, concat_axis=0, tiled=True)  12.4 us
    all_to_all x1, waiting for transfers between devices, shards(): lax.all_to_all(expert_sum.astype(jnp.bfloat16), 'ep', split_axis=0, conca...  10.8 us
    all_to_all x1, starting transfers between devices, sum_at_owner(): parts = lax.all_to_all(cut_along(array, dim, size), axis, 0, 0, tiled=True)  7.34 us
    all_to_all x1, starting transfers between devices, shards(): lax.all_to_all(expert_sum.astype(jnp.bfloat16), 'ep', split_axis=0, conca...  4.98 us
    unnamed x33, local copies, waits for them, and re-layouts  4.15 us
  transfers between devices with their start and end apart: 3, of which 3 were waited for; matrix products, arithmetic and copies ran while one was open for 2% of the time, Pallas kernels for 0%

commit v1 on v0

v1 whole, which is shorter than its diff:
```python
import functools

import jax
import jax.numpy as jnp
from jax import lax
from jax.experimental import pallas as pl
from jax.experimental.pallas import tpu as pltpu
from jax.sharding import PartitionSpec as P

EPS = 1e-06
NX = 4
MESH = pl.DeviceIdType.MESH
NT = (((1,), (1,)), ((), ()))
bf16, f32, i32 = jnp.bfloat16, jnp.float32, jnp.int32
SLOT = 144
LANES = 256


def wrap(v, n):
    return jnp.where(v < 0, v + n, v)


def mm(a, b):
    return jnp.dot(a, b, preferred_element_type=f32)


def mm_nt(a, b):
    return lax.dot_general(a, b, NT, preferred_element_type=f32)


def kernel(
    n_ep, n_tp,
    tok, again, wq, wk, wv, ow, lam, hgain, ck, cv, lens, mgain, gwt, uwt, dw, sgt, sut, sd, ids, ew,
    out,
    tok_v, wqkv, k_v, v_v, ow_v, wt, dcat, lam_s, lens_s, again_v, hgain_v, mgain_v, ids_v, ew_v,
    x_s, tokblk, idp, ewp, dnt, gainb,
    send1, recv1, send2, recv2, xt, pt, sib, q5, recv5, send6, recv6,
    lsem, ssem, rsem, s3, r3, f3s, f3r, s5a, r5a, s5, r5,
):
    n_z, n_y = n_ep // NX, n_tp // 2
    seqs, width = tok.shape
    cache = ck.shape[1]
    me_ep, me_tp = lax.axis_index("ep"), lax.axis_index("tp")
    z, x = me_ep // NX, lax.rem(me_ep, NX)
    y, c = me_tp // 2, lax.rem(me_tp, 2)

    def ep_at(slot):
        dz, dx = slot // NX, slot % NX
        return lax.rem(z + dz, n_z) * NX + lax.rem(x + dx, NX)

    def ep_back(slot):
        dz, dx = slot // NX, slot % NX
        return lax.rem(z + n_z - dz, n_z) * NX + lax.rem(x + NX - dx, NX)

    bar = pltpu.get_barrier_semaphore()
    for r in range(1, n_tp):
        pl.semaphore_signal(bar, inc=1, device_id={"tp": lax.rem(me_tp + r, n_tp)}, device_id_type=MESH)

    def greet(i, carry):
        pl.semaphore_signal(bar, inc=1, device_id={"ep": ep_at(i)}, device_id_type=MESH)
        return carry

    loads = []

    def load(src, dst):
        cp = pltpu.make_async_copy(src, dst, lsem.at[len(loads)])
        cp.start()
        loads.append(cp)
        return cp

    c_tok = [load(tok, tok_v), load(again, again_v)]
    c_qkv = [load(w, wqkv.at[:, pl.ds(128 * i, 128)]) for i, w in enumerate((wq, wk, wv))]
    c_len = [load(lens, lens_s), load(lam, lam_s), load(hgain, hgain_v)]
    c_k = [load(ck.at[s], k_v.at[s // 2, :, pl.ds(128 * (s % 2), 128)]) for s in range(seqs)]
    c_v = [load(cv.at[s], v_v.at[s // 2, :, pl.ds(128 * (s % 2), 128)]) for s in range(seqs)]
    c_ow = [load(ow.at[pl.ds(SLOT * t, SLOT)], ow_v.at[t, pl.ds(0, SLOT)]) for t in range(n_tp)]
    lax.fori_loop(1, n_ep, greet, 0)
    c_ids = [load(ids, ids_v), load(ew, ew_v), load(mgain, mgain_v)]
    c_wt = [load(w, wt.at[pl.ds(64 * i, 64)]) for i, w in enumerate((gwt, uwt, sgt, sut))]
    c_dn = [load(w, dcat.at[pl.ds(64 * i, 64)]) for i, w in enumerate((dw, sd))]

    def done(cps):
        for cp in cps:
            cp.wait()

    x_s[...] = jnp.zeros_like(x_s)
    if seqs % 2:
        k_v[seqs // 2, :, pl.ds(128, 128)] = jnp.zeros((cache, 128), bf16)
        v_v[seqs // 2, :, pl.ds(128, 128)] = jnp.zeros((cache, 128), bf16)
    done(c_tok)
    x_s[0:seqs, :] = tok_v[...].astype(f32)
    xv = x_s[...]
    gain = again_v[...].astype(f32).reshape(1, width)
    normed = (xv * lax.rsqrt(jnp.mean(xv * xv, axis=-1, keepdims=True) + EPS) * gain).astype(bf16)
    done(c_qkv)
    qkv = mm(normed, wqkv[...]).astype(bf16).astype(f32)
    q, kn, vn = qkv[:, 0:128], qkv[:, 128:256], qkv[:, 256:384]
    lane = lax.broadcasted_iota(i32, (8, 128), 1)
    first = lane < 64
    qk = q * kn
    scale = 0.125
    own = jnp.concatenate(
        [jnp.sum(jnp.where(first, qk, 0.0), axis=-1, keepdims=True),
         jnp.sum(jnp.where(first, 0.0, qk), axis=-1, keepdims=True)], axis=0) * scale
    q2 = jnp.concatenate([jnp.where(first, q, 0.0), jnp.where(first, 0.0, q)], axis=0)
    row16 = lax.broadcasted_iota(i32, (16, 128), 0)
    row16 = jnp.where(row16 >= 8, row16 - 8, row16)
    scores = jnp.zeros((16, cache), f32)
    done(c_len)
    for p in range((seqs + 1) // 2):
        done(c_k[2 * p : 2 * p + 2])
        qa = jnp.where(row16 == 2 * p, q2, 0.0)
        qb = jnp.where(row16 == 2 * p + 1, q2, 0.0)
        scores += mm_nt(jnp.concatenate([qa, qb], axis=1).astype(bf16), k_v[p])
    scores = scores * scale
    rcol = lax.broadcasted_iota(i32, (16, 1), 0)
    rcol = jnp.where(rcol >= 8, rcol - 8, rcol)
    lcol = jnp.zeros((16, 1), i32)
    for s in range(seqs):
        lcol = jnp.where(rcol == s, lens_s[s], lcol)
    live = lax.broadcasted_iota(i32, (16, cache), 1) < lcol
    peak = jnp.maximum(jnp.max(jnp.where(live, scores, -jnp.inf), axis=-1, keepdims=True), own)
    terms = jnp.where(live, jnp.exp(scores - peak), 0.0)
    own_term = jnp.exp(own - peak)
    inv = 1.0 / (jnp.sum(terms, axis=-1, keepdims=True) + own_term)
    probs, own_prob = terms * inv, own_term * inv
    lm = lam_s[0]
    mix = (probs[0:8] - lm * probs[8:16]).astype(bf16).astype(f32)
    own_mix = (own_prob[0:8] - lm * own_prob[8:16]).astype(bf16).astype(f32)
    rowc = lax.broadcasted_iota(i32, (8, cache), 0)
    both = jnp.zeros((8, 256), f32)
    for p in range((seqs + 1) // 2):
        done(c_v[2 * p : 2 * p + 2])
        both += mm(jnp.where(rowc // 2 == p, mix, 0.0).astype(bf16), v_v[p])
    row8 = lax.broadcasted_iota(i32, (8, 128), 0)
    head = jnp.where(row8 % 2 == 0, both[:, 0:128], both[:, 128:256]) + own_mix * vn
    hg = hgain_v[...].astype(f32).reshape(1, 128)
    head_n = (head * lax.rsqrt(jnp.mean(head * head, axis=-1, keepdims=True) + EPS) * hg).astype(bf16)
    done(c_ow)
    part = mm_nt(head_n, ow_v[...].reshape(n_tp * LANES, 128)).astype(bf16)
    for t in range(n_tp):
        send1[t] = part[:, LANES * t : LANES * (t + 1)]

    pl.semaphore_wait(bar, n_tp - 1 + n_ep - 1)
    for r in sorted(range(1, n_tp), key=lambda r: -min(r, n_tp - r)):
        to = lax.rem(me_tp + r, n_tp)
        pltpu.make_async_remote_copy(
            src_ref=send1.at[to], dst_ref=recv1.at[r - 1], send_sem=ssem.at[0], recv_sem=rsem.at[0],
            device_id={"tp": to}, device_id_type=MESH).start()

    for t in range(n_tp):
        tokblk[t, :, pl.ds(0, SLOT)] = xv[:, SLOT * t : SLOT * (t + 1)]
    done(c_ids)
    idp[...] = jnp.full_like(idp, -1)
    ewp[...] = jnp.zeros_like(ewp)
    idp[0:seqs, 0 : ids.shape[1]] = ids_v[...]
    ewp[0:seqs, 0 : ids.shape[1]] = ew_v[...]
    idv, ewv = idp[...], ewp[...]
    rid = wrap((idv >> 2) - z, n_z) * NX + wrap((idv & 3) - x, NX)
    rid = jnp.where(idv < 0, -1, rid)
    slot_l, rank_l = lane >> 1, lane & 1
    hit, wsum = jnp.zeros((8, 128), f32), jnp.zeros((8, 128), f32)
    for k in range(ids.shape[1]):
        m = rid[:, k : k + 1] == slot_l
        hit = jnp.where(m, 1.0, hit)
        wsum = jnp.where(m, ewv[:, k : k + 1], wsum)
    rank = jnp.zeros((8, 128), f32)
    for s in range(seqs):
        rank += jnp.where(row8 > s, hit[s : s + 1, :], 0.0)
    place = jnp.where(rank == rank_l.astype(f32), hit, 0.0)
    comb = place * wsum
    comb_hi = comb.astype(bf16)
    comb_lo = (comb - comb_hi.astype(f32)).astype(bf16)
    comb2 = jnp.concatenate([comb_hi.astype(f32), comb_lo.astype(f32)], axis=0).astype(bf16)
    place_t = jnp.concatenate([place, jnp.zeros((120, 128), f32)], axis=0).T.astype(bf16)
    done(c_dn)
    for i in range(width // 128):
        cols = pl.ds(128 * i, 128)
        dnt[cols, :] = dcat[:, cols].astype(f32).T.astype(bf16)
    mg = mgain_v[...].astype(f32).reshape(1, width)
    for i in range(width // 128):
        gainb[pl.ds(128 * i, 128), :] = jnp.broadcast_to(mg[:, 128 * i : 128 * (i + 1)], (128, 128)).T

    own_part = send1[me_tp].astype(f32)
    own_tok = tokblk[me_tp]
    pltpu.make_async_copy(recv1, recv1, rsem.at[0]).wait()
    attn = own_part + jnp.sum(recv1[...].astype(f32), axis=0)
    lane2 = lax.broadcasted_iota(i32, (8, LANES), 1)
    mixed = jnp.where(lane2 < SLOT, own_tok + attn, 0.0).astype(bf16)
    mixed_f = mixed.astype(f32)

    mixed_p = jnp.concatenate([mixed_f, jnp.zeros((120, LANES), f32)], axis=0).astype(bf16)
    rows = mm(place_t, mixed_p)[0 : 2 * n_ep].astype(bf16)
    send2[...] = rows.reshape(n_ep, 2, LANES)

    def give(i, carry):
        slot = n_ep - i
        pltpu.make_async_remote_copy(
            src_ref=send2.at[slot], dst_ref=recv2.at[slot], send_sem=ssem.at[1], recv_sem=rsem.at[1],
            device_id={"ep": ep_at(slot)}, device_id_type=MESH).start()
        return carry

    lax.fori_loop(1, n_ep, give, 0)
    recv2[0] = send2[0]
    done(c_wt)
    pltpu.make_async_copy(recv2.at[pl.ds(1, n_ep - 1)], recv2.at[pl.ds(1, n_ep - 1)], rsem.at[1]).wait()
    got = recv2[...].reshape(2 * n_ep, LANES).astype(f32)
    parts = [got, mixed_f]
    if 128 - 2 * n_ep - 8 > 0:
        parts.append(jnp.zeros((128 - 2 * n_ep - 8, LANES), f32))
    rows_t = jnp.concatenate(parts, axis=0).T
    xt[me_tp] = rows_t[0:SLOT].astype(bf16)

    def gather_copy(dy):
        return pltpu.make_async_remote_copy(
            src_ref=xt.at[me_tp], dst_ref=xt.at[me_tp], send_sem=s3.at[dy], recv_sem=r3.at[dy],
            device_id={"tp": lax.rem(y + dy, n_y) * 2 + c}, device_id_type=MESH)

    def hand_copy(dy):
        t = lax.rem(y + n_y - dy, n_y) * 2 + c
        return pltpu.make_async_remote_copy(
            src_ref=xt.at[t], dst_ref=xt.at[t], send_sem=f3s.at[dy], recv_sem=f3r.at[dy],
            device_id={"tp": y * 2 + 1 - c}, device_id_type=MESH)

    far = sorted(range(1, n_y), key=lambda d: -min(d, n_y - d))
    for dy in far:
        gather_copy(dy).start()
    hand_copy(0).start()
    for dy in reversed(far):
        gather_copy(dy).wait_recv()
        hand_copy(dy).start()
    for dy in range(n_y):
        hand_copy(dy).wait_recv()

    xa = xt[...].reshape(width, 128).astype(f32)
    inv_rms = lax.rsqrt(jnp.sum(xa * xa, axis=0, keepdims=True) * (1.0 / width) + EPS)
    xn = (xa * inv_rms * gainb[...]).astype(bf16)
    hid = mm(wt[...], xn)
    ge, ue, gs, us = hid[0:64], hid[64:128], hid[128:192], hid[192:256]
    lane64 = lax.broadcasted_iota(i32, (64, 128), 1)
    routed_l = lane64 < 2 * n_ep
    he = jnp.where(routed_l, ge / (1.0 + jnp.exp(-ge)) * ue, 0.0)
    hs = jnp.where(routed_l, 0.0, gs / (1.0 + jnp.exp(-gs)) * us)
    hcat = jnp.concatenate([he, hs], axis=0).astype(bf16)

    def sib_copy(v):
        t = v * 2 + 1 - c
        return pltpu.make_async_remote_copy(
            src_ref=pt.at[t], dst_ref=sib.at[v], send_sem=s5a.at[v], recv_sem=r5a.at[v],
            device_id={"tp": y * 2 + 1 - c}, device_id_type=MESH)

    def sum_copy(dy):
        v = lax.rem(y + dy, n_y)
        return pltpu.make_async_remote_copy(
            src_ref=q5.at[v], dst_ref=recv5.at[dy], send_sem=s5.at[dy], recv_sem=r5.at[dy],
            device_id={"tp": v * 2 + c}, device_id_type=MESH)

    pt[...] = mm(dnt[...], hcat).astype(bf16).reshape(n_tp, SLOT, 128)
    order = far + [0]
    for dy in order:
        sib_copy(lax.rem(y + dy, n_y)).start()
    for dy in order:
        v = lax.rem(y + dy, n_y)
        sib_copy(v).wait_recv()
        pair = pt[v * 2 + c].astype(f32) + sib[v].astype(f32)
        if dy:
            q5[v] = pair.astype(bf16)
            sum_copy(dy).start()
        else:
            total = pair
    for dy in reversed(far):
        sum_copy(dy).wait_recv()
        total += recv5[dy].astype(f32)
    back = jnp.concatenate([total, jnp.zeros((LANES - SLOT, 128), f32)], axis=0).T
    shared = back[2 * n_ep : 2 * n_ep + 8]
    send6[...] = back[0 : 2 * n_ep].astype(bf16).reshape(n_ep, 2, LANES)

    def give_back(i, carry):
        slot = n_ep - i
        pltpu.make_async_remote_copy(
            src_ref=send6.at[slot], dst_ref=recv6.at[slot], send_sem=ssem.at[2], recv_sem=rsem.at[2],
            device_id={"ep": ep_back(slot)}, device_id_type=MESH).start()
        return carry

    lax.fori_loop(1, n_ep, give_back, 0)
    recv6[0] = send6[0]
    pltpu.make_async_copy(recv1, recv1, ssem.at[0]).wait()
    pltpu.make_async_copy(recv2.at[pl.ds(1, n_ep - 1)], recv2.at[pl.ds(1, n_ep - 1)], ssem.at[1]).wait()
    for dy in range(n_y):
        hand_copy(dy).wait_send()
        sib_copy(dy).wait_send()
        if dy:
            gather_copy(dy).wait_send()
            sum_copy(dy).wait_send()
    pltpu.make_async_copy(recv6.at[pl.ds(1, n_ep - 1)], recv6.at[pl.ds(1, n_ep - 1)], rsem.at[2]).wait()
    vals = recv6[...].reshape(2 * n_ep, LANES)
    two = mm(comb2[:, 0 : 2 * n_ep], vals)
    res = mixed_f + (two[0:8] + two[8:16]) + shared
    out[...] = res[0:seqs, 0:SLOT].astype(bf16)
    pltpu.make_async_copy(recv6.at[pl.ds(1, n_ep - 1)], recv6.at[pl.ds(1, n_ep - 1)], ssem.at[2]).wait()


def solution(mesh):
    n_ep, n_tp = mesh.shape["ep"], mesh.shape["tp"]
    n_y = n_tp // 2

    def step(tokens, attn_gain, wq, wk, wv, ow, lambdas, head_gain, ck, cv, lengths, moe_gain,
             gw, uw, dw, sg, su, sd, ids, ew):
        seqs, width = tokens.shape
        cache = ck.shape[1]
        pairs = (seqs + 1) // 2
        V, DMA = pltpu.VMEM, pltpu.SemaphoreType.DMA
        scratch = [
            V((seqs, width), bf16), V((width, 384), bf16), V((pairs, cache, 256), bf16), V((pairs, cache, 256), bf16),
            V((n_tp, LANES, 128), bf16), V((256, width), bf16), V((128, width), bf16),
            pltpu.SMEM((1,), f32), pltpu.SMEM((seqs,), i32), V((width,), bf16), V((128,), bf16), V((width,), bf16),
            V(ids.shape, i32), V(ew.shape, f32),
            V((8, width), f32), V((n_tp, 8, LANES), f32), V((8, 128), i32), V((8, 128), f32),
            V((width, 128), bf16), V((width, 128), f32),
            V((n_tp, 8, LANES), bf16), V((n_tp - 1, 8, LANES), bf16),
            V((n_ep, 2, LANES), bf16), V((n_ep, 2, LANES), bf16),
            V((n_tp, SLOT, 128), bf16), V((n_tp, SLOT, 128), bf16), V((n_y, SLOT, 128), bf16),
            V((n_y, SLOT, 128), bf16), V((n_y, SLOT, 128), bf16),
            V((n_ep, 2, LANES), bf16), V((n_ep, 2, LANES), bf16),
            DMA((64,)), DMA((3,)), DMA((3,)),
            DMA((n_y,)), DMA((n_y,)), DMA((n_y,)), DMA((n_y,)),
            DMA((n_y,)), DMA((n_y,)), DMA((n_y,)), DMA((n_y,)),
        ]
        return pl.pallas_call(
            functools.partial(kernel, n_ep, n_tp),
            out_shape=jax.ShapeDtypeStruct((seqs, width // n_tp), bf16),
            in_specs=[pl.BlockSpec(memory_space=pl.ANY)] * 20,
            out_specs=pl.BlockSpec(memory_space=pltpu.VMEM),
            scratch_shapes=scratch,
            compiler_params=pltpu.CompilerParams(collective_id=0, has_side_effects=True),
            name="decode_step",
        )(tokens, attn_gain, wq, wk, wv, ow, lambdas, head_gain,
          ck.reshape(seqs, cache, 128), cv.reshape(seqs, cache, 128), lengths, moe_gain,
          gw[0].T, uw[0].T, dw[0], sg.T, su.T, sd, ids, ew)

    in_specs = (
        P("ep", None), P(), P(None, "tp"), P(None, "tp"), P(None, "tp"), P(None, "tp"), P("tp"), P(),
        P("ep", None, "tp", None), P("ep", None, "tp", None), P("ep"), P(),
        P("ep", None, "tp"), P("ep", None, "tp"), P("ep", "tp", None),
        P(None, "tp"), P(None, "tp"), P("tp", None), P("ep", None), P("ep", None),
    )
    return jax.shard_map(step, mesh=mesh, in_specs=in_specs, out_specs=P("ep", "tp"), check_vma=False)
```

time: 122 us -> 64.6 us (0.53)
  Pallas kernels: 0 us -> 62.5 us
  waiting for transfers between devices: 48.2 us -> 0 us
  blocking collectives: 26.3 us -> 0 us
  starting transfers between devices: 24.7 us -> 0 us
  matrix products: 9.57 us -> 0 us
  local copies, waits for them, and re-layouts: 7.72 us -> 1.28 us
  other arithmetic: 3.79 us -> 0 us
    pallas_call x0 -> x1, Pallas kernels: none -> 62.5 us  [step(): pl.pallas_call(functools.partial(kernel, n_ep, n_tp), out_shape=jax.Shape...]
    all_to_all x3 -> x0, waiting for transfers between devices: 48.2 us -> none  [the longest x1 18.9 us: shards(): lax.all_to_all(send_rows, 'ep', split_axis=0, concat_axis=0, tiled=True)]
    all_gather x1 -> x0, blocking collectives: 26.3 us -> none  [over_pieces(): return lax.all_gather(array, axis).astype(jnp.float32).sum(0)]
    all_to_all x3 -> x0, starting transfers between devices: 24.7 us -> none  [the longest x1 12.4 us: shards(): lax.all_to_all(send_rows, 'ep', split_axis=0, concat_axis=0, tiled=True)]
    dot_general x12 -> x0, matrix products: 9.57 us -> none  [the longest x1 1.92 us: shards(): jnp.einsum('shmd,sjhmd->shmj', queries, past_keys, preferred_element_type...]
    unnamed x33 -> x1, local copies, waits for them, and re-layouts: 4.15 us -> 1.28 us
    all_to_all x4 -> x0, local copies, waits for them, and re-layouts: 1.81 us -> none  [the longest x2 1.1 us: shards(): lax.all_to_all(send_rows, 'ep', split_axis=0, concat_axis=0, tiled=True)]
    reduce_sum x7 -> x0, other arithmetic: 1.73 us -> none  [the longest x2 1.03 us: rms_scale(): jnp.mean(wide * wide, axis=-1, keepdims=True) + epsilon]
  transfers between devices with their start and end apart: 3 -> 0, of which waited for: 3 -> 0; matrix products, arithmetic and copies ran while one was open for 2% -> 0% of each run, Pallas kernels for 0% -> 0%
where the time goes in v1:
time: 64.6 us; the launch traced here: 64.4 us
  Pallas kernels  62.5 us (97%)
  local copies, waits for them, and re-layouts  1.28 us (2%)
  between operations  0.66 us (1%)
    pallas_call x1, Pallas kernels, step(): pl.pallas_call(functools.partial(kernel, n_ep, n_tp), out_shape=jax.Shape...  62.5 us

profile of v1, /device:TPU:1, one launch (start us, length us, event | category | flops | bytes accessed | tf_op | source)
XLA Modules:
  0.0 64.4 jit_solution(11872045002170398509)
XLA Ops:
  0.7 62.5 %decode_step.1 = bf16[7,144]{1,0:T(8,128)(2,1)} custom-call(bf16[7,2304]{1,0:T(8,128)(2,1)} %tok.1, bf16[2304]{0:T(1024)(128)(2,1)} %again.1, bf16[2304,128]{1,0:T(8,128)(2,1)} %wq.1, bf16[2304,128]{1,0:T(8,128)(2,1)} %wk.1, bf16[2304,128]{1,0:T(8,128)(2,1)} %wv.1, bf16[2304,128]{1,0:T(8,128)(2,1)} %ow.1, f32[1]{0:T(128)S(6)} %copy.22.lam, ...), custom_call_target="tpu_custom_call" | custom-call | tf_op jit(solution)/shard_map/decode_step/pallas_call | solution.py:329
  63.2 1.3 %copy.23 = bf16[7,144]{1,0:T(8,128)(2,1)} copy(bf16[7,144]{1,0:T(8,128)(2,1)} %decode_step.1) | data formatting | bytes 4032

commit v2 on v1

--- a/solution.py
+++ b/solution.py
@@ -14,6 +14,8 @@
 bf16, f32, i32 = jnp.bfloat16, jnp.float32, jnp.int32
 SLOT = 144
 LANES = 256
+REST = SLOT - 128
+PAIR = 384
 
 
 def wrap(v, n):
@@ -33,9 +35,9 @@
     tok, again, wq, wk, wv, ow, lam, hgain, ck, cv, lens, mgain, gwt, uwt, dw, sgt, sut, sd, ids, ew,
     out,
     tok_v, wqkv, k_v, v_v, ow_v, wt, dcat, lam_s, lens_s, again_v, hgain_v, mgain_v, ids_v, ew_v,
-    x_s, tokblk, idp, ewp, dnt, gainb,
-    send1, recv1, send2, recv2, xt, pt, sib, q5, recv5, send6, recv6,
-    lsem, ssem, rsem, s3, r3, f3s, f3r, s5a, r5a, s5, r5,
+    x_s, tokblk, idp, ewp, dnt, dsib, gainb,
+    send1, recv1, send2, recv2, xt, q5, recv5, send6, recv6,
+    lsem, ssem, rsem, s3, r3, f3s, f3r, s5, r5, wsem,
 ):
     n_z, n_y = n_ep // NX, n_tp // 2
     seqs, width = tok.shape
@@ -44,22 +46,26 @@
     z, x = me_ep // NX, lax.rem(me_ep, NX)
     y, c = me_tp // 2, lax.rem(me_tp, 2)
 
+    half = n_tp // 2
+    pair = lax.rem(me_tp, half)
+    other = lax.rem(me_tp + half, n_tp)
+    sibling = {"tp": y * 2 + 1 - c}
+    z_at = [wrap(z + d - n_z, n_z) * NX for d in range(n_z)]
+    x_at = [wrap(x + d - NX, NX) for d in range(NX)]
+
+    def hops(slot):
+        dz, dx = slot // NX, slot % NX
+        return min(dz, n_z - dz) + min(dx, NX - dx)
+
+    slots = sorted(range(1, n_ep), key=lambda s: -hops(s))
+
     def ep_at(slot):
-        dz, dx = slot // NX, slot % NX
-        return lax.rem(z + dz, n_z) * NX + lax.rem(x + dx, NX)
+        return z_at[slot // NX] + x_at[slot % NX]
 
     def ep_back(slot):
-        dz, dx = slot // NX, slot % NX
-        return lax.rem(z + n_z - dz, n_z) * NX + lax.rem(x + NX - dx, NX)
+        return z_at[-(slot // NX) % n_z] + x_at[-(slot % NX) % NX]
 
     bar = pltpu.get_barrier_semaphore()
-    for r in range(1, n_tp):
-        pl.semaphore_signal(bar, inc=1, device_id={"tp": lax.rem(me_tp + r, n_tp)}, device_id_type=MESH)
-
-    def greet(i, carry):
-        pl.semaphore_signal(bar, inc=1, device_id={"ep": ep_at(i)}, device_id_type=MESH)
-        return carry
-
     loads = []
 
     def load(src, dst):
@@ -70,11 +76,18 @@
 
     c_tok = [load(tok, tok_v), load(again, again_v)]
     c_qkv = [load(w, wqkv.at[:, pl.ds(128 * i, 128)]) for i, w in enumerate((wq, wk, wv))]
+    for r in range(1, n_tp):
+        pl.semaphore_signal(bar, inc=1, device_id={"tp": lax.rem(me_tp + r, n_tp)}, device_id_type=MESH)
     c_len = [load(lens, lens_s), load(lam, lam_s), load(hgain, hgain_v)]
     c_k = [load(ck.at[s], k_v.at[s // 2, :, pl.ds(128 * (s % 2), 128)]) for s in range(seqs)]
     c_v = [load(cv.at[s], v_v.at[s // 2, :, pl.ds(128 * (s % 2), 128)]) for s in range(seqs)]
-    c_ow = [load(ow.at[pl.ds(SLOT * t, SLOT)], ow_v.at[t, pl.ds(0, SLOT)]) for t in range(n_tp)]
-    lax.fori_loop(1, n_ep, greet, 0)
+    c_ow = []
+    for t in range(n_tp):
+        hi = t // half
+        c_ow.append(load(ow.at[pl.ds(SLOT * t, 128)], ow_v.at[t % half, pl.ds(128 * hi, 128)]))
+        c_ow.append(load(ow.at[pl.ds(SLOT * t + 128, REST)], ow_v.at[t % half, pl.ds(256 + REST * hi, REST)]))
+    for slot in slots:
+        pl.semaphore_signal(bar, inc=1, device_id={"ep": ep_at(slot)}, device_id_type=MESH)
     c_ids = [load(ids, ids_v), load(ew, ew_v), load(mgain, mgain_v)]
     c_wt = [load(w, wt.at[pl.ds(64 * i, 64)]) for i, w in enumerate((gwt, uwt, sgt, sut))]
     c_dn = [load(w, dcat.at[pl.ds(64 * i, 64)]) for i, w in enumerate((dw, sd))]
@@ -137,19 +150,21 @@
     hg = hgain_v[...].astype(f32).reshape(1, 128)
     head_n = (head * lax.rsqrt(jnp.mean(head * head, axis=-1, keepdims=True) + EPS) * hg).astype(bf16)
     done(c_ow)
-    part = mm_nt(head_n, ow_v[...].reshape(n_tp * LANES, 128)).astype(bf16)
-    for t in range(n_tp):
-        send1[t] = part[:, LANES * t : LANES * (t + 1)]
+    part = mm_nt(head_n, ow_v[...].reshape(half * PAIR, 128)).astype(bf16)
+    for p in range(half):
+        send1[p] = part[:, PAIR * p : PAIR * (p + 1)]
 
     pl.semaphore_wait(bar, n_tp - 1 + n_ep - 1)
     for r in sorted(range(1, n_tp), key=lambda r: -min(r, n_tp - r)):
         to = lax.rem(me_tp + r, n_tp)
         pltpu.make_async_remote_copy(
-            src_ref=send1.at[to], dst_ref=recv1.at[r - 1], send_sem=ssem.at[0], recv_sem=rsem.at[0],
+            src_ref=send1.at[lax.rem(to, half)], dst_ref=recv1.at[r - 1], send_sem=ssem.at[0], recv_sem=rsem.at[0],
             device_id={"tp": to}, device_id_type=MESH).start()
 
     for t in range(n_tp):
-        tokblk[t, :, pl.ds(0, SLOT)] = xv[:, SLOT * t : SLOT * (t + 1)]
+        hi = t // half
+        tokblk[t % half, :, pl.ds(128 * hi, 128)] = xv[:, SLOT * t : SLOT * t + 128]
+        tokblk[t % half, :, pl.ds(256 + REST * hi, REST)] = xv[:, SLOT * t + 128 : SLOT * (t + 1)]
     done(c_ids)
     idp[...] = jnp.full_like(idp, -1)
     ewp[...] = jnp.zeros_like(ewp)
@@ -176,78 +191,94 @@
     done(c_dn)
     for i in range(width // 128):
         cols = pl.ds(128 * i, 128)
-        dnt[cols, :] = dcat[:, cols].astype(f32).T.astype(bf16)
+        chunk = dcat[:, cols].astype(f32).T.astype(bf16)
+        at = 128 * i
+        while at < 128 * (i + 1):
+            t, o = at // SLOT, at % SLOT
+            n = min(SLOT - o, 128 * (i + 1) - at)
+            dnt[t, pl.ds(o, n), :] = chunk[at - 128 * i : at - 128 * i + n]
+            at += n
     mg = mgain_v[...].astype(f32).reshape(1, width)
     for i in range(width // 128):
         gainb[pl.ds(128 * i, 128), :] = jnp.broadcast_to(mg[:, 128 * i : 128 * (i + 1)], (128, 128)).T
 
-    own_part = send1[me_tp].astype(f32)
-    own_tok = tokblk[me_tp]
+    own_part = send1[pair].astype(f32)
+    own_tok = tokblk[pair]
     pltpu.make_async_copy(recv1, recv1, rsem.at[0]).wait()
     attn = own_part + jnp.sum(recv1[...].astype(f32), axis=0)
-    lane2 = lax.broadcasted_iota(i32, (8, LANES), 1)
-    mixed = jnp.where(lane2 < SLOT, own_tok + attn, 0.0).astype(bf16)
+    lane2 = lax.broadcasted_iota(i32, (8, PAIR), 1)
+    mixed = jnp.where(lane2 < 2 * SLOT, own_tok + attn, 0.0).astype(bf16)
     mixed_f = mixed.astype(f32)
 
-    mixed_p = jnp.concatenate([mixed_f, jnp.zeros((120, LANES), f32)], axis=0).astype(bf16)
+    mixed_p = jnp.concatenate([mixed_f, jnp.zeros((120, PAIR), f32)], axis=0).astype(bf16)
     rows = mm(place_t, mixed_p)[0 : 2 * n_ep].astype(bf16)
-    send2[...] = rows.reshape(n_ep, 2, LANES)
-
-    def give(i, carry):
-        slot = n_ep - i
+    send2[...] = rows.reshape(n_ep, 2, PAIR)
+
+    for slot in slots:
         pltpu.make_async_remote_copy(
             src_ref=send2.at[slot], dst_ref=recv2.at[slot], send_sem=ssem.at[1], recv_sem=rsem.at[1],
             device_id={"ep": ep_at(slot)}, device_id_type=MESH).start()
-        return carry
-
-    lax.fori_loop(1, n_ep, give, 0)
     recv2[0] = send2[0]
     done(c_wt)
+    w_copy = pltpu.make_async_remote_copy(
+        src_ref=wt.at[pl.ds(0, 256)], dst_ref=wt.at[pl.ds(256, 256)], send_sem=wsem.at[0], recv_sem=wsem.at[1],
+        device_id=sibling, device_id_type=MESH)
+    w_copy.start()
+    for v in range(n_y):
+        pltpu.make_async_remote_copy(
+            src_ref=dnt.at[v * 2 + 1 - c], dst_ref=dsib.at[v], send_sem=wsem.at[2], recv_sem=wsem.at[3],
+            device_id=sibling, device_id_type=MESH).start()
     pltpu.make_async_copy(recv2.at[pl.ds(1, n_ep - 1)], recv2.at[pl.ds(1, n_ep - 1)], rsem.at[1]).wait()
-    got = recv2[...].reshape(2 * n_ep, LANES).astype(f32)
-    parts = [got, mixed_f]
-    if 128 - 2 * n_ep - 8 > 0:
-        parts.append(jnp.zeros((128 - 2 * n_ep - 8, LANES), f32))
-    rows_t = jnp.concatenate(parts, axis=0).T
-    xt[me_tp] = rows_t[0:SLOT].astype(bf16)
-
-    def gather_copy(dy):
+    got = recv2[...].reshape(2 * n_ep, PAIR).astype(f32)
+    rows_t = jnp.concatenate([got, mixed_f, jnp.zeros((120 - 2 * n_ep, PAIR), f32)], axis=0).T.astype(bf16)
+    for hi in range(2):
+        xt[pair + half * hi, pl.ds(0, 128), :] = rows_t[128 * hi : 128 * hi + 128]
+        xt[pair + half * hi, pl.ds(128, REST), :] = rows_t[256 + REST * hi : 256 + REST * (hi + 1)]
+
+    moves = [(2, 0), (n_y - 2, 0), (1, 0), (n_y - 1, 0), (1, half), (n_y - 1, half)]
+
+    def gather_copy(k):
+        dy, off = moves[k]
+        t = lax.rem(me_tp + off, n_tp)
         return pltpu.make_async_remote_copy(
-            src_ref=xt.at[me_tp], dst_ref=xt.at[me_tp], send_sem=s3.at[dy], recv_sem=r3.at[dy],
-            device_id={"tp": lax.rem(y + dy, n_y) * 2 + c}, device_id_type=MESH)
-
-    def hand_copy(dy):
-        t = lax.rem(y + n_y - dy, n_y) * 2 + c
+            src_ref=xt.at[t], dst_ref=xt.at[t], send_sem=s3.at[k], recv_sem=r3.at[k],
+            device_id={"tp": lax.rem(me_tp + 2 * dy, n_tp)}, device_id_type=MESH)
+
+    def hand_copy(k):
+        if k < len(moves):
+            dy, off = moves[k]
+            t = lax.rem(me_tp + 2 * (n_y - dy) + off, n_tp)
+        else:
+            t = (me_tp, other)[k - len(moves)]
         return pltpu.make_async_remote_copy(
-            src_ref=xt.at[t], dst_ref=xt.at[t], send_sem=f3s.at[dy], recv_sem=f3r.at[dy],
-            device_id={"tp": y * 2 + 1 - c}, device_id_type=MESH)
-
-    far = sorted(range(1, n_y), key=lambda d: -min(d, n_y - d))
-    for dy in far:
-        gather_copy(dy).start()
-    hand_copy(0).start()
-    for dy in reversed(far):
-        gather_copy(dy).wait_recv()
-        hand_copy(dy).start()
-    for dy in range(n_y):
-        hand_copy(dy).wait_recv()
+            src_ref=xt.at[t], dst_ref=xt.at[t], send_sem=f3s.at[k], recv_sem=f3r.at[k],
+            device_id=sibling, device_id_type=MESH)
+
+    for k in range(len(moves)):
+        gather_copy(k).start()
+    hand_copy(len(moves)).start()
+    hand_copy(len(moves) + 1).start()
+    for k in (2, 3, 4, 5, 0, 1):
+        gather_copy(k).wait_recv()
+        hand_copy(k).start()
+    pltpu.make_async_copy(wt.at[pl.ds(256, 256)], wt.at[pl.ds(256, 256)], wsem.at[1]).wait()
+    pltpu.make_async_copy(dsib, dsib, wsem.at[3]).wait()
+    for k in range(len(moves) + 2):
+        hand_copy(k).wait_recv()
 
     xa = xt[...].reshape(width, 128).astype(f32)
     inv_rms = lax.rsqrt(jnp.sum(xa * xa, axis=0, keepdims=True) * (1.0 / width) + EPS)
     xn = (xa * inv_rms * gainb[...]).astype(bf16)
     hid = mm(wt[...], xn)
-    ge, ue, gs, us = hid[0:64], hid[64:128], hid[128:192], hid[192:256]
-    lane64 = lax.broadcasted_iota(i32, (64, 128), 1)
-    routed_l = lane64 < 2 * n_ep
-    he = jnp.where(routed_l, ge / (1.0 + jnp.exp(-ge)) * ue, 0.0)
-    hs = jnp.where(routed_l, 0.0, gs / (1.0 + jnp.exp(-gs)) * us)
-    hcat = jnp.concatenate([he, hs], axis=0).astype(bf16)
-
-    def sib_copy(v):
-        t = v * 2 + 1 - c
-        return pltpu.make_async_remote_copy(
-            src_ref=pt.at[t], dst_ref=sib.at[v], send_sem=s5a.at[v], recv_sem=r5a.at[v],
-            device_id={"tp": y * 2 + 1 - c}, device_id_type=MESH)
+    routed_l = lax.broadcasted_iota(i32, (64, 128), 1) < 2 * n_ep
+    parts = []
+    for o in (0, 256):
+        ge, ue, gs, us = (hid[o + 64 * i : o + 64 * (i + 1)] for i in range(4))
+        parts.append(jnp.where(routed_l, ge / (1.0 + jnp.exp(-ge)) * ue, 0.0))
+        parts.append(jnp.where(routed_l, 0.0, gs / (1.0 + jnp.exp(-gs)) * us))
+    hcat = jnp.concatenate(parts, axis=0).astype(bf16)
+
+    far = sorted(range(1, n_y), key=lambda d: -min(d, n_y - d))
 
     def sum_copy(dy):
         v = lax.rem(y + dy, n_y)
@@ -255,19 +286,14 @@
             src_ref=q5.at[v], dst_ref=recv5.at[dy], send_sem=s5.at[dy], recv_sem=r5.at[dy],
             device_id={"tp": v * 2 + c}, device_id_type=MESH)
 
-    pt[...] = mm(dnt[...], hcat).astype(bf16).reshape(n_tp, SLOT, 128)
-    order = far + [0]
-    for dy in order:
-        sib_copy(lax.rem(y + dy, n_y)).start()
-    for dy in order:
+    for dy in far + [0]:
         v = lax.rem(y + dy, n_y)
-        sib_copy(v).wait_recv()
-        pair = pt[v * 2 + c].astype(f32) + sib[v].astype(f32)
+        term = mm(jnp.concatenate([dnt[v * 2 + c], dsib[v]], axis=1), hcat)
         if dy:
-            q5[v] = pair.astype(bf16)
+            q5[v] = term.astype(bf16)
             sum_copy(dy).start()
         else:
-            total = pair
+            total = term
     for dy in reversed(far):
         sum_copy(dy).wait_recv()
         total += recv5[dy].astype(f32)
@@ -275,34 +301,36 @@
     shared = back[2 * n_ep : 2 * n_ep + 8]
     send6[...] = back[0 : 2 * n_ep].astype(bf16).reshape(n_ep, 2, LANES)
 
-    def give_back(i, carry):
-        slot = n_ep - i
+    for slot in slots:
         pltpu.make_async_remote_copy(
             src_ref=send6.at[slot], dst_ref=recv6.at[slot], send_sem=ssem.at[2], recv_sem=rsem.at[2],
             device_id={"ep": ep_back(slot)}, device_id_type=MESH).start()
-        return carry
-
-    lax.fori_loop(1, n_ep, give_back, 0)
     recv6[0] = send6[0]
     pltpu.make_async_copy(recv1, recv1, ssem.at[0]).wait()
     pltpu.make_async_copy(recv2.at[pl.ds(1, n_ep - 1)], recv2.at[pl.ds(1, n_ep - 1)], ssem.at[1]).wait()
-    for dy in range(n_y):
-        hand_copy(dy).wait_send()
-        sib_copy(dy).wait_send()
-        if dy:
-            gather_copy(dy).wait_send()
-            sum_copy(dy).wait_send()
+    w_copy.wait_send()
+    pltpu.make_async_copy(dsib, dsib, wsem.at[2]).wait()
+    for k in range(len(moves) + 2):
+        hand_copy(k).wait_send()
+        if k < len(moves):
+            gather_copy(k).wait_send()
+    for dy in far:
+        sum_copy(dy).wait_send()
     pltpu.make_async_copy(recv6.at[pl.ds(1, n_ep - 1)], recv6.at[pl.ds(1, n_ep - 1)], rsem.at[2]).wait()
     vals = recv6[...].reshape(2 * n_ep, LANES)
     two = mm(comb2[:, 0 : 2 * n_ep], vals)
-    res = mixed_f + (two[0:8] + two[8:16]) + shared
+    hi = y >= n_y // 2
+    mine = jnp.concatenate(
+        [jnp.where(hi, mixed_f[:, 128:256], mixed_f[:, 0:128]),
+         jnp.where(hi, pltpu.roll(mixed_f[:, 256:384], 128 - REST, 1), mixed_f[:, 256:384])], axis=1)
+    res = mine + (two[0:8] + two[8:16]) + shared
     out[...] = res[0:seqs, 0:SLOT].astype(bf16)
     pltpu.make_async_copy(recv6.at[pl.ds(1, n_ep - 1)], recv6.at[pl.ds(1, n_ep - 1)], ssem.at[2]).wait()
 
 
 def solution(mesh):
     n_ep, n_tp = mesh.shape["ep"], mesh.shape["tp"]
-    n_y = n_tp // 2
+    n_y = half = n_tp // 2
 
     def step(tokens, attn_gain, wq, wk, wv, ow, lambdas, head_gain, ck, cv, lengths, moe_gain,
              gw, uw, dw, sg, su, sd, ids, ew):
@@ -312,19 +340,17 @@
         V, DMA = pltpu.VMEM, pltpu.SemaphoreType.DMA
         scratch = [
             V((seqs, width), bf16), V((width, 384), bf16), V((pairs, cache, 256), bf16), V((pairs, cache, 256), bf16),
-            V((n_tp, LANES, 128), bf16), V((256, width), bf16), V((128, width), bf16),
+            V((half, PAIR, 128), bf16), V((512, width), bf16), V((128, width), bf16),
             pltpu.SMEM((1,), f32), pltpu.SMEM((seqs,), i32), V((width,), bf16), V((128,), bf16), V((width,), bf16),
             V(ids.shape, i32), V(ew.shape, f32),
-            V((8, width), f32), V((n_tp, 8, LANES), f32), V((8, 128), i32), V((8, 128), f32),
-            V((width, 128), bf16), V((width, 128), f32),
-            V((n_tp, 8, LANES), bf16), V((n_tp - 1, 8, LANES), bf16),
+            V((8, width), f32), V((half, 8, PAIR), f32), V((8, 128), i32), V((8, 128), f32),
+            V((n_tp, SLOT, 128), bf16), V((n_y, SLOT, 128), bf16), V((width, 128), f32),
+            V((half, 8, PAIR), bf16), V((n_tp - 1, 8, PAIR), bf16),
+            V((n_ep, 2, PAIR), bf16), V((n_ep, 2, PAIR), bf16),
+            V((n_tp, SLOT, 128), bf16), V((n_y, SLOT, 128), bf16), V((n_y, SLOT, 128), bf16),
             V((n_ep, 2, LANES), bf16), V((n_ep, 2, LANES), bf16),
-            V((n_tp, SLOT, 128), bf16), V((n_tp, SLOT, 128), bf16), V((n_y, SLOT, 128), bf16),
-            V((n_y, SLOT, 128), bf16), V((n_y, SLOT, 128), bf16),
-            V((n_ep, 2, LANES), bf16), V((n_ep, 2, LANES), bf16),
-            DMA((64,)), DMA((3,)), DMA((3,)),
-            DMA((n_y,)), DMA((n_y,)), DMA((n_y,)), DMA((n_y,)),
-            DMA((n_y,)), DMA((n_y,)), DMA((n_y,)), DMA((n_y,)),
+            DMA((72,)), DMA((3,)), DMA((3,)),
+            DMA((n_y,)), DMA((n_y,)), DMA((n_y,)), DMA((n_y,)), DMA((n_y,)), DMA((n_y,)), DMA((4,)),
         ]
         return pl.pallas_call(
             functools.partial(kernel, n_ep, n_tp),

time: 64.6 us -> 59.7 us (0.924)
  Pallas kernels: 62.5 us -> 57.6 us
    pallas_call x1, Pallas kernels: 62.5 us -> 57.6 us  [step(): pl.pallas_call(functools.partial(kernel, n_ep, n_tp), out_shape=jax.Shape...]
where the time goes in v2:
time: 59.7 us; the launch traced here: 59.5 us
  Pallas kernels  57.6 us (96%)
  local copies, waits for them, and re-layouts  1.28 us (2%)
  between operations  0.66 us (1%)
    pallas_call x1, Pallas kernels, step(): pl.pallas_call(functools.partial(kernel, n_ep, n_tp), out_shape=jax.Shape...  57.6 us
    unnamed x1, local copies, waits for them, and re-layouts  1.28 us

profile of v2, /device:TPU:1, one launch (start us, length us, event | category | flops | bytes accessed | tf_op | source)
XLA Modules:
  0.0 59.5 jit_solution(8689677278900724363)
XLA Ops:
  0.7 57.6 %decode_step.1 = bf16[7,144]{1,0:T(8,128)(2,1)} custom-call(bf16[7,2304]{1,0:T(8,128)(2,1)} %tok.1, bf16[2304]{0:T(1024)(128)(2,1)} %again.1, bf16[2304,128]{1,0:T(8,128)(2,1)} %wq.1, bf16[2304,128]{1,0:T(8,128)(2,1)} %wk.1, bf16[2304,128]{1,0:T(8,128)(2,1)} %wv.1, bf16[2304,128]{1,0:T(8,128)(2,1)} %ow.1, f32[1]{0:T(128)S(6)} %copy.22.lam, ...), custom_call_target="tpu_custom_call" | custom-call | tf_op jit(solution)/shard_map/decode_step/pallas_call | solution.py:355
  58.3 1.3 %copy.23 = bf16[7,144]{1,0:T(8,128)(2,1)} copy(bf16[7,144]{1,0:T(8,128)(2,1)} %decode_step.1) | data formatting | bytes 4032

commit v3 on v2

v3 whole, which is shorter than its diff:
```python
import functools

import jax
import jax.numpy as jnp
from jax import lax
from jax.experimental import pallas as pl
from jax.experimental.pallas import tpu as pltpu
from jax.sharding import PartitionSpec as P

EPS = 1e-06
NX = 4
MESH = pl.DeviceIdType.MESH
NT = (((1,), (1,)), ((), ()))
bf16, f32, i32 = jnp.bfloat16, jnp.float32, jnp.int32
SLOT = 144
LANES = 256
BLOCK = 2 * SLOT
PAIR = 384
HEADK = 256
TAILK = BLOCK - HEADK


def wrap(v, n):
    return jnp.where(v < 0, v + n, v)


def mm(a, b):
    return jnp.dot(a, b, preferred_element_type=f32)


def mm_nt(a, b):
    return lax.dot_general(a, b, NT, preferred_element_type=f32)


def kernel(
    n_ep, n_tp,
    tok, again, wq, wk, wv, ow, lam, hgain, ck, cv, lens, mgain, gwt, uwt, dw, sgt, sut, sd, ids, ew,
    out,
    tok_v, wqkv, k_v, v_v, ow_v, wt, dcat, lam_v, lens_s, again_v, hgain_v, mgain_v, ids_v, ew_v,
    x_s, tokblk, idp, ewp, dnt, dsib, wp,
    send1, recv1, send2, recv2, xt, q5, recv5, send6, recv6, share_s, share_r,
    lsem, ssem, rsem, r3, f3r, wsem, hsem,
):
    n_z, n_y = n_ep // NX, n_tp // 2
    seqs, width = tok.shape
    cache = ck.shape[1]
    me_ep, me_tp = lax.axis_index("ep"), lax.axis_index("tp")
    z, x = me_ep // NX, lax.rem(me_ep, NX)
    y, c = me_tp // 2, lax.rem(me_tp, 2)

    half = n_tp // 2
    pair = lax.rem(me_tp, half)
    other = lax.rem(me_tp + half, n_tp)
    sibling = {"tp": y * 2 + 1 - c}
    above, below = lax.rem(me_tp + 2, n_tp), lax.rem(me_tp + n_tp - 2, n_tp)
    z_at = [wrap(z + d - n_z, n_z) * NX for d in range(n_z)]
    x_at = [wrap(x + d - NX, NX) for d in range(NX)]

    def hops(slot):
        dz, dx = slot // NX, slot % NX
        return min(dz, n_z - dz) + min(dx, NX - dx)

    slots = sorted(range(1, n_ep), key=lambda s: -hops(s))

    def ep_at(slot):
        return z_at[slot // NX] + x_at[slot % NX]

    def ep_back(slot):
        return z_at[-(slot // NX) % n_z] + x_at[-(slot % NX) % NX]

    bar = pltpu.get_barrier_semaphore()
    groups = []

    def load(pairs, region=None):
        sem = lsem.at[len(groups)]
        for src, dst in pairs:
            pltpu.make_async_copy(src, dst, sem).start()
        groups.append(region)
        region = pairs[0][1] if region is None else region
        return lambda: whole(region, sem)

    def whole(ref, sem):
        pltpu.make_async_copy(ref, ref, sem).wait()

    def cached(src, dst):
        return [
            load([(src.at[s], dst.at[p, :, pl.ds(128 * (s % 2), 128)]) for s in range(2 * p, min(2 * p + 2, seqs))],
                 dst.at[p, :, pl.ds(0, 128 * min(2, seqs - 2 * p))])
            for p in range((seqs + 1) // 2)]

    c_tok, c_gain = load([(tok, tok_v)]), load([(again, again_v)])
    step = width // 3
    c_qkv = [
        load([(w.at[pl.ds(step * j, step)], wqkv.at[pl.ds(step * j, step), pl.ds(128 * i, 128)])
              for i, w in enumerate((wq, wk, wv))], wqkv.at[pl.ds(step * j, step)])
        for j in range(3)]
    for slot in slots:
        pl.semaphore_signal(bar, inc=1, device_id={"ep": ep_at(slot), "tp": above}, device_id_type=MESH)
        pl.semaphore_signal(bar, inc=1, device_id={"ep": ep_at(slot)}, device_id_type=MESH)
    for r in range(1, n_tp):
        pl.semaphore_signal(bar, inc=1, device_id={"tp": lax.rem(me_tp + r, n_tp)}, device_id_type=MESH)
    c_k = cached(ck, k_v)
    c_len, c_lam, c_hgain = load([(lens, lens_s)]), load([(lam, lam_v)]), load([(hgain, hgain_v)])
    c_v = cached(cv, v_v)
    c_ow = load(
        [(ow.at[pl.ds(SLOT * t, SLOT)], ow_v.at[t % half, pl.ds(SLOT * (t // half), SLOT)]) for t in range(n_tp)],
        ow_v.at[:, pl.ds(0, BLOCK)])
    c_ids, c_ew, c_mgain = load([(ids, ids_v)]), load([(ew, ew_v)]), load([(mgain, mgain_v)])
    c_dn = load([(w, dcat.at[pl.ds(64 * i, 64)]) for i, w in enumerate((dw, sd))], dcat)
    c_wt = load([(w, wt.at[pl.ds(64 * i, 64)]) for i, w in enumerate((gwt, uwt, sgt, sut))], wt)

    x_s[...] = jnp.zeros_like(x_s)
    if seqs % 2:
        k_v[seqs // 2, :, pl.ds(128, 128)] = jnp.zeros((cache, 128), bf16)
        v_v[seqs // 2, :, pl.ds(128, 128)] = jnp.zeros((cache, 128), bf16)
    c_tok()
    c_gain()
    x_s[0:seqs, :] = tok_v[...].astype(f32)
    xv = x_s[...]
    gain = again_v[...].astype(f32).reshape(1, width)
    normed = (xv * lax.rsqrt(jnp.mean(xv * xv, axis=-1, keepdims=True) + EPS) * gain).astype(bf16)
    qkv = jnp.zeros((8, 384), f32)
    for j in range(3):
        c_qkv[j]()
        qkv += mm(normed[:, step * j : step * (j + 1)], wqkv[pl.ds(step * j, step), :])
    qkv = qkv.astype(bf16).astype(f32)
    q, kn, vn = qkv[:, 0:128], qkv[:, 128:256], qkv[:, 256:384]
    lane = lax.broadcasted_iota(i32, (8, 128), 1)
    first = lane < 64
    qk = q * kn
    scale = 0.125
    own = jnp.concatenate(
        [jnp.sum(jnp.where(first, qk, 0.0), axis=-1, keepdims=True),
         jnp.sum(jnp.where(first, 0.0, qk), axis=-1, keepdims=True)], axis=0) * scale
    q2 = jnp.concatenate([jnp.where(first, q, 0.0), jnp.where(first, 0.0, q)], axis=0)
    row16 = lax.broadcasted_iota(i32, (16, 128), 0)
    row16 = jnp.where(row16 >= 8, row16 - 8, row16)
    scores = jnp.zeros((16, cache), f32)
    c_len()
    c_lam()
    c_hgain()
    for p in range((seqs + 1) // 2):
        c_k[p]()
        qa = jnp.where(row16 == 2 * p, q2, 0.0)
        qb = jnp.where(row16 == 2 * p + 1, q2, 0.0)
        scores += mm_nt(jnp.concatenate([qa, qb], axis=1).astype(bf16), k_v[p])
    scores = scores * scale
    rcol = lax.broadcasted_iota(i32, (16, 1), 0)
    rcol = jnp.where(rcol >= 8, rcol - 8, rcol)
    lcol = jnp.zeros((16, 1), i32)
    for s in range(seqs):
        lcol = jnp.where(rcol == s, lens_s[s], lcol)
    live = lax.broadcasted_iota(i32, (16, cache), 1) < lcol
    peak = jnp.maximum(jnp.max(jnp.where(live, scores, -jnp.inf), axis=-1, keepdims=True), own)
    terms = jnp.where(live, jnp.exp(scores - peak), 0.0)
    own_term = jnp.exp(own - peak)
    inv = 1.0 / (jnp.sum(terms, axis=-1, keepdims=True) + own_term)
    probs, own_prob = terms * inv, own_term * inv
    lm = lam_v[...]
    mix = (probs[0:8] - lm * probs[8:16]).astype(bf16).astype(f32)
    own_mix = (own_prob[0:8] - lm * own_prob[8:16]).astype(bf16).astype(f32)
    rowc = lax.broadcasted_iota(i32, (8, cache), 0)
    both = jnp.zeros((8, 256), f32)
    for p in range((seqs + 1) // 2):
        c_v[p]()
        both += mm(jnp.where(rowc // 2 == p, mix, 0.0).astype(bf16), v_v[p])
    row8 = lax.broadcasted_iota(i32, (8, 128), 0)
    head = jnp.where(row8 % 2 == 0, both[:, 0:128], both[:, 128:256]) + own_mix * vn
    hg = hgain_v[...].astype(f32).reshape(1, 128)
    head_n = (head * lax.rsqrt(jnp.mean(head * head, axis=-1, keepdims=True) + EPS) * hg).astype(bf16)
    c_ow()
    part = mm_nt(head_n, ow_v[...].reshape(half * PAIR, 128)).astype(bf16)
    for p in range(half):
        send1[p] = part[:, PAIR * p : PAIR * (p + 1)]

    pl.semaphore_wait(bar, n_tp - 1 + 2 * (n_ep - 1))
    for r in sorted(range(1, n_tp), key=lambda r: -min(r, n_tp - r)):
        to = lax.rem(me_tp + r, n_tp)
        pltpu.make_async_remote_copy(
            src_ref=send1.at[lax.rem(to, half)], dst_ref=recv1.at[r - 1], send_sem=ssem.at[0], recv_sem=rsem.at[0],
            device_id={"tp": to}, device_id_type=MESH).start()

    for p in range(half):
        q0, q1 = SLOT * p, SLOT * (p + half)
        tokblk[p] = jnp.concatenate(
            [xv[:, q0 : q0 + SLOT], xv[:, q1 : q1 + SLOT], jnp.zeros((8, PAIR - BLOCK), f32)], axis=1)
    c_ids()
    c_ew()
    c_mgain()
    idp[...] = jnp.full_like(idp, -1)
    ewp[...] = jnp.zeros_like(ewp)
    idp[0:seqs, 0 : ids.shape[1]] = ids_v[...]
    ewp[0:seqs, 0 : ids.shape[1]] = ew_v[...]
    idv, ewv = idp[...], ewp[...]
    rid = wrap((idv >> 2) - z, n_z) * NX + wrap((idv & 3) - x, NX)
    rid = jnp.where(idv < 0, -1, rid)
    slot_l, rank_l = lane >> 1, lane & 1
    hit, wsum = jnp.zeros((8, 128), f32), jnp.zeros((8, 128), f32)
    for k in range(ids.shape[1]):
        m = rid[:, k : k + 1] == slot_l
        hit = jnp.where(m, 1.0, hit)
        wsum = jnp.where(m, ewv[:, k : k + 1], wsum)
    rank = jnp.zeros((8, 128), f32)
    for s in range(seqs):
        rank += jnp.where(row8 > s, hit[s : s + 1, :], 0.0)
    place = jnp.where(rank == rank_l.astype(f32), hit, 0.0)
    comb = place * wsum
    comb_hi = comb.astype(bf16)
    comb_lo = (comb - comb_hi.astype(f32)).astype(bf16)
    comb2 = jnp.concatenate([comb_hi.astype(f32), comb_lo.astype(f32)], axis=0).astype(bf16)
    place_t = jnp.concatenate([place, jnp.zeros((120, 128), f32)], axis=0).T.astype(bf16)
    c_dn()
    for i in range(width // 128):
        cols = pl.ds(128 * i, 128)
        chunk = dcat[:, cols].astype(f32).T.astype(bf16)
        at = 128 * i
        while at < 128 * (i + 1):
            t, o = at // SLOT, at % SLOT
            n = min(SLOT - o, 128 * (i + 1) - at)
            dnt[t, pl.ds(o, n), :] = chunk[at - 128 * i : at - 128 * i + n]
            at += n
    mg = mgain_v[...].astype(f32).reshape(1, width)
    c_wt()
    for i in range(4):
        rows = pl.ds(64 * i, 64)
        w = wt[rows, :].astype(f32) * mg
        tails = []
        for p in range(half):
            q0, q1 = SLOT * p, SLOT * (p + half)
            wp[p, rows, :] = jnp.concatenate(
                [w[:, q0 : q0 + SLOT], w[:, q1 : q1 + HEADK - SLOT]], axis=1).astype(bf16)
            tails.append(w[:, q1 + HEADK - SLOT : q1 + SLOT])
        wp[half, rows, :] = jnp.concatenate(tails, axis=1).astype(bf16)
    own_part = send1[pair].astype(f32)
    own_tok = tokblk[pair]
    whole(recv1, rsem.at[0])
    attn = own_part + jnp.sum(recv1[...].astype(f32), axis=0)
    lane2 = lax.broadcasted_iota(i32, (8, PAIR), 1)
    mixed = jnp.where(lane2 < BLOCK, own_tok + attn, 0.0).astype(bf16)
    mixed_f = mixed.astype(f32)

    mixed_p = jnp.concatenate([mixed_f, jnp.zeros((120, PAIR), f32)], axis=0).astype(bf16)
    rows = mm(place_t, mixed_p)[0 : 2 * n_ep].astype(bf16)
    send2[...] = rows.reshape(n_ep, 2, PAIR)

    for slot in slots:
        pltpu.make_async_remote_copy(
            src_ref=send2.at[slot], dst_ref=recv2.at[slot], send_sem=ssem.at[1], recv_sem=rsem.at[1],
            device_id={"ep": ep_at(slot)}, device_id_type=MESH).start()
    recv2[0] = send2[0]
    w_copy = pltpu.make_async_remote_copy(
        src_ref=wp.at[:, pl.ds(0, 256)], dst_ref=wp.at[:, pl.ds(256, 256)], send_sem=wsem.at[0],
        recv_sem=wsem.at[1], device_id=sibling, device_id_type=MESH)
    w_copy.start()
    for v in range(n_y):
        pltpu.make_async_remote_copy(
            src_ref=dnt.at[v * 2 + 1 - c], dst_ref=dsib.at[v], send_sem=wsem.at[2], recv_sem=wsem.at[3],
            device_id=sibling, device_id_type=MESH).start()
    pltpu.make_async_copy(recv2.at[pl.ds(1, n_ep - 1)], recv2.at[pl.ds(1, n_ep - 1)], rsem.at[1]).wait()
    got = recv2[...].reshape(2 * n_ep, PAIR).astype(f32)
    rows_t = jnp.concatenate([got, mixed_f, jnp.zeros((120 - 2 * n_ep, PAIR), f32)], axis=0).T
    xt[pair] = rows_t[0:BLOCK].astype(bf16)

    upper = y // (n_y // 2)

    moves = (2, n_y - 2, 1, n_y - 1)
    hands = moves + (0,)

    def pair_at(dy, core):
        return lax.rem(y + dy, n_y // 2) * 2 + core

    def gather_copy(dy):
        if dy in (1, n_y - 1):
            part = xt.at[pair]
        else:
            part = xt.at[pair, pl.ds(pl.multiple_of(upper * SLOT, 16), SLOT)]
        return pltpu.make_async_remote_copy(
            src_ref=part, dst_ref=part, send_sem=ssem.at[4], recv_sem=r3.at[moves.index(dy)],
            device_id={"tp": lax.rem(me_tp + 2 * dy, n_tp)}, device_id_type=MESH)

    def hand_copy(dy):
        from_y = lax.rem(y + n_y - dy, n_y)
        if dy in (0, 1, n_y - 1):
            part = xt.at[pair_at(n_y - dy, c)]
        else:
            part = xt.at[pair_at(n_y - dy, c), pl.ds(pl.multiple_of(from_y // (n_y // 2) * SLOT, 16), SLOT)]
        return pltpu.make_async_remote_copy(
            src_ref=part, dst_ref=part, send_sem=ssem.at[5], recv_sem=f3r.at[hands.index(dy)],
            device_id=sibling, device_id_type=MESH)

    def products(dy, core):
        p = pair_at(n_y - dy, core)
        block = xt[p]
        wide = block.astype(f32)
        return mm(wp[p], block[0:HEADK]), jnp.sum(wide * wide, axis=0, keepdims=True)

    for dy in moves:
        gather_copy(dy).start()
    hand_copy(0).start()
    pltpu.make_async_copy(wp.at[:, pl.ds(256, 256)], wp.at[:, pl.ds(256, 256)], wsem.at[1]).wait()
    hid, squares = products(0, c)
    for dy in (1, n_y - 1):
        gather_copy(dy).wait_recv()
        hand_copy(dy).start()
    for dy in (1, n_y - 1):
        more = products(dy, c)
        hid, squares = hid + more[0], squares + more[1]
    hand_copy(0).wait_recv()
    more = products(0, 1 - c)
    hid, squares = hid + more[0], squares + more[1]
    for dy in (2, n_y - 2):
        gather_copy(dy).wait_recv()
        hand_copy(dy).start()
    more = products(2, c)
    hid, squares = hid + more[0], squares + more[1]
    for dy in (1, n_y - 1):
        hand_copy(dy).wait_recv()
        more = products(dy, 1 - c)
        hid, squares = hid + more[0], squares + more[1]
    whole(dsib, wsem.at[3])
    for dy in (2, n_y - 2):
        hand_copy(dy).wait_recv()
    more = products(2, 1 - c)
    hid, squares = hid + more[0], squares + more[1]
    tails = jnp.concatenate([xt[p, pl.ds(HEADK, TAILK), :] for p in range(half)], axis=0)
    hid = (hid + mm(wp[half], tails)) * lax.rsqrt(squares * (1.0 / width) + EPS)
    routed_l = lax.broadcasted_iota(i32, (64, 128), 1) < 2 * n_ep
    parts = []
    for o in (0, 256):
        ge, ue, gs, us = (hid[o + 64 * i : o + 64 * (i + 1)] for i in range(4))
        parts.append(jnp.where(routed_l, ge / (1.0 + jnp.exp(-ge)) * ue, 0.0))
        parts.append(jnp.where(routed_l, 0.0, gs / (1.0 + jnp.exp(-gs)) * us))
    hcat = jnp.concatenate(parts, axis=0).astype(bf16)

    far = (3, n_y - 3, 2, n_y - 2, 1, n_y - 1)
    far_at = {dy: i for i, dy in enumerate(far)}

    def sum_copy(dy):
        to = lax.rem(y + dy, n_y)
        v = to if dy < n_y // 2 else lax.rem(to + n_y - 1, n_y)
        return pltpu.make_async_remote_copy(
            src_ref=q5.at[v], dst_ref=recv5.at[far_at[dy]], send_sem=ssem.at[6], recv_sem=rsem.at[4],
            device_id={"tp": to * 2 + c}, device_id_type=MESH)

    def terms(v):
        return mm(jnp.concatenate([dnt[v * 2 + c], dsib[v]], axis=1), hcat)

    for dy in far:
        to = lax.rem(y + dy, n_y)
        v = to if dy < n_y // 2 else lax.rem(to + n_y - 1, n_y)
        q5[v] = terms(v).astype(bf16)
        sum_copy(dy).start()
    totals = [terms(y), terms(lax.rem(y + n_y - 1, n_y))]
    whole(recv5, rsem.at[4])
    for dy in far:
        side = 0 if dy < n_y // 2 else 1
        totals[side] += recv5[far_at[dy]].astype(f32)
    backs = [jnp.concatenate([a, jnp.zeros((LANES - SLOT, 128), f32)], axis=0).T for a in totals]
    shared = backs[0][2 * n_ep : 2 * n_ep + 8]
    share_s[...] = backs[1][2 * n_ep : 2 * n_ep + 8]
    for side in range(2):
        send6[side] = backs[side][0 : 2 * n_ep].astype(bf16).reshape(n_ep, 2, LANES)

    for slot in slots + [0]:
        for side in (1, 0) if slot else (1,):
            pltpu.make_async_remote_copy(
                src_ref=send6.at[side, slot], dst_ref=recv6.at[side, slot],
                send_sem=ssem.at[2 + side], recv_sem=rsem.at[2 + side],
                device_id={"ep": ep_back(slot), "tp": below if side else me_tp}, device_id_type=MESH).start()
    share_copy = pltpu.make_async_remote_copy(
        src_ref=share_s, dst_ref=share_r, send_sem=hsem.at[0], recv_sem=hsem.at[1],
        device_id={"tp": below}, device_id_type=MESH)
    share_copy.start()
    recv6[0, 0] = send6[0, 0]
    whole(recv1, ssem.at[0])
    pltpu.make_async_copy(recv2.at[pl.ds(1, n_ep - 1)], recv2.at[pl.ds(1, n_ep - 1)], ssem.at[1]).wait()
    w_copy.wait_send()
    whole(dsib, wsem.at[2])
    whole(xt.at[pl.ds(0, 3)], ssem.at[4])
    whole(xt.at[pl.ds(0, 4)], ssem.at[5])
    whole(recv5, ssem.at[6])
    share_copy.wait_recv()
    whole(recv6.at[0, pl.ds(1, n_ep - 1)], rsem.at[2])
    whole(recv6.at[1], rsem.at[3])
    shared = shared + share_r[...]
    two = sum(mm(comb2[:, 0 : 2 * n_ep], recv6[side].reshape(2 * n_ep, LANES)) for side in range(2))
    mine = jnp.where(y >= n_y // 2, mixed_f[:, SLOT : BLOCK], mixed_f[:, 0:SLOT])
    res = mine + ((two[0:8] + two[8:16]) + shared)[:, 0:SLOT]
    out[...] = res[0:seqs].astype(bf16)
    whole(recv6.at[0, pl.ds(1, n_ep - 1)], ssem.at[2])
    whole(recv6.at[1], ssem.at[3])
    share_copy.wait_send()


def solution(mesh):
    n_ep, n_tp = mesh.shape["ep"], mesh.shape["tp"]
    n_y = half = n_tp // 2

    def step(tokens, attn_gain, wq, wk, wv, ow, lambdas, head_gain, ck, cv, lengths, moe_gain,
             gw, uw, dw, sg, su, sd, ids, ew):
        seqs, width = tokens.shape
        cache = ck.shape[1]
        pairs = (seqs + 1) // 2
        V, DMA = pltpu.VMEM, pltpu.SemaphoreType.DMA
        scratch = [
            V((seqs, width), bf16), V((width, 384), bf16), V((pairs, cache, 256), bf16), V((pairs, cache, 256), bf16),
            V((half, PAIR, 128), bf16), V((256, width), bf16), V((128, width), bf16),
            V((1, 1), f32), pltpu.SMEM((seqs,), i32), V((width,), bf16), V((128,), bf16), V((width,), bf16),
            V(ids.shape, i32), V(ew.shape, f32),
            V((8, width), f32), V((half, 8, PAIR), f32), V((8, 128), i32), V((8, 128), f32),
            V((n_tp, SLOT, 128), bf16), V((n_y, SLOT, 128), bf16), V((half + 1, 512, HEADK), bf16),
            V((half, 8, PAIR), bf16), V((n_tp - 1, 8, PAIR), bf16),
            V((n_ep, 2, PAIR), bf16), V((n_ep, 2, PAIR), bf16),
            V((half, BLOCK, 128), bf16), V((n_y, SLOT, 128), bf16), V((n_y - 2, SLOT, 128), bf16),
            V((2, n_ep, 2, LANES), bf16), V((2, n_ep, 2, LANES), bf16), V((8, LANES), f32), V((8, LANES), f32),
            DMA((24,)), DMA((7,)), DMA((5,)), DMA((4,)), DMA((5,)), DMA((4,)), DMA((2,)),
        ]
        return pl.pallas_call(
            functools.partial(kernel, n_ep, n_tp),
            out_shape=pltpu.VMEM((seqs, width // n_tp), bf16),
            in_specs=[pl.BlockSpec(memory_space=pl.ANY)] * 20,
            out_specs=pl.BlockSpec(memory_space=pltpu.VMEM),
            scratch_shapes=scratch,
            compiler_params=pltpu.CompilerParams(collective_id=0, has_side_effects=True),
            name="decode_step",
        )(tokens, attn_gain, wq, wk, wv, ow, lambdas.reshape(1, 1), head_gain,
          ck.reshape(seqs, cache, 128), cv.reshape(seqs, cache, 128), lengths, moe_gain,
          gw[0].T, uw[0].T, dw[0], sg.T, su.T, sd, ids, ew)

    in_specs = (
        P("ep", None), P(), P(None, "tp"), P(None, "tp"), P(None, "tp"), P(None, "tp"), P("tp"), P(),
        P("ep", None, "tp", None), P("ep", None, "tp", None), P("ep"), P(),
        P("ep", None, "tp"), P("ep", None, "tp"), P("ep", "tp", None),
        P(None, "tp"), P(None, "tp"), P("tp", None), P("ep", None), P("ep", None),
    )
    return jax.shard_map(step, mesh=mesh, in_specs=in_specs, out_specs=P("ep", "tp"), check_vma=False)
```

time: 59.7 us -> 57.5 us (0.963)
  Pallas kernels: 57.6 us -> 56.1 us
  local copies, waits for them, and re-layouts: 1.28 us -> 0.6 us
    pallas_call x1, Pallas kernels: 57.6 us -> 56.1 us  [step(): pl.pallas_call(functools.partial(kernel, n_ep, n_tp), out_shape=pltpu.VME...]
    unnamed x1, local copies, waits for them, and re-layouts: 1.28 us -> 0.6 us
where the time goes in v3:
time: 57.5 us; the launch traced here: 57.4 us
  Pallas kernels  56.1 us (98%)
  between operations  0.66 us (1%)
  local copies, waits for them, and re-layouts  0.6 us (1%)
    pallas_call x1, Pallas kernels, step(): pl.pallas_call(functools.partial(kernel, n_ep, n_tp), out_shape=pltpu.VME...  56.1 us

profile of v3, /device:TPU:1, one launch (start us, length us, event | category | flops | bytes accessed | tf_op | source)
XLA Modules:
  0.0 57.4 jit_solution(3654033787443417052)
XLA Ops:
  0.7 56.1 %decode_step.1 = bf16[7,144]{1,0:T(8,128)(2,1)S(1)} custom-call(bf16[7,2304]{1,0:T(8,128)(2,1)} %tok.1, bf16[2304]{0:T(1024)(128)(2,1)} %again.1, bf16[2304,128]{1,0:T(8,128)(2,1)} %wq.1, bf16[2304,128]{1,0:T(8,128)(2,1)} %wk.1, bf16[2304,128]{1,0:T(8,128)(2,1)} %wv.1, bf16[2304,128]{1,0:T(8,128)(2,1)} %ow.1, f32[1,1]{1,0:T(1,128)} %bitcast.12.lam, ...), custom_call_target="tpu_custom_call" | custom-call | tf_op jit(solution)/shard_map/decode_step/pallas_call | solution.py:418
  56.8 0.6 %copy.22 = bf16[7,144]{1,0:T(8,128)(2,1)} copy(bf16[7,144]{1,0:T(8,128)(2,1)S(1)} %decode_step.1) | data formatting | bytes 4032

commit v4 on v3

--- a/solution.py
+++ b/solution.py
@@ -16,6 +16,7 @@
 LANES = 256
 BLOCK = 2 * SLOT
 PAIR = 384
+FOLD = 120
 HEADK = 256
 TAILK = BLOCK - HEADK
 
@@ -37,7 +38,7 @@
     tok, again, wq, wk, wv, ow, lam, hgain, ck, cv, lens, mgain, gwt, uwt, dw, sgt, sut, sd, ids, ew,
     out,
     tok_v, wqkv, k_v, v_v, ow_v, wt, dcat, lam_v, lens_s, again_v, hgain_v, mgain_v, ids_v, ew_v,
-    x_s, tokblk, idp, ewp, dnt, dsib, wp,
+    x_s, tokblk, idp, ewp, dnt, drem, dsib, dsibr, wp,
     send1, recv1, send2, recv2, xt, q5, recv5, send6, recv6, share_s, share_r,
     lsem, ssem, rsem, r3, f3r, wsem, hsem,
 ):
@@ -52,7 +53,7 @@
     pair = lax.rem(me_tp, half)
     other = lax.rem(me_tp + half, n_tp)
     sibling = {"tp": y * 2 + 1 - c}
-    above, below = lax.rem(me_tp + 2, n_tp), lax.rem(me_tp + n_tp - 2, n_tp)
+    below = lax.rem(me_tp + n_tp - 2, n_tp)
     z_at = [wrap(z + d - n_z, n_z) * NX for d in range(n_z)]
     x_at = [wrap(x + d - NX, NX) for d in range(NX)]
 
@@ -88,17 +89,16 @@
                  dst.at[p, :, pl.ds(0, 128 * min(2, seqs - 2 * p))])
             for p in range((seqs + 1) // 2)]
 
+    for slot in slots:
+        pl.semaphore_signal(bar, inc=1, device_id={"ep": ep_at(slot)}, device_id_type=MESH)
+    for r in range(1, n_tp):
+        pl.semaphore_signal(bar, inc=1, device_id={"tp": lax.rem(me_tp + r, n_tp)}, device_id_type=MESH)
     c_tok, c_gain = load([(tok, tok_v)]), load([(again, again_v)])
     step = width // 3
     c_qkv = [
         load([(w.at[pl.ds(step * j, step)], wqkv.at[pl.ds(step * j, step), pl.ds(128 * i, 128)])
               for i, w in enumerate((wq, wk, wv))], wqkv.at[pl.ds(step * j, step)])
         for j in range(3)]
-    for slot in slots:
-        pl.semaphore_signal(bar, inc=1, device_id={"ep": ep_at(slot), "tp": above}, device_id_type=MESH)
-        pl.semaphore_signal(bar, inc=1, device_id={"ep": ep_at(slot)}, device_id_type=MESH)
-    for r in range(1, n_tp):
-        pl.semaphore_signal(bar, inc=1, device_id={"tp": lax.rem(me_tp + r, n_tp)}, device_id_type=MESH)
     c_k = cached(ck, k_v)
     c_len, c_lam, c_hgain = load([(lens, lens_s)]), load([(lam, lam_v)]), load([(hgain, hgain_v)])
     c_v = cached(cv, v_v)
@@ -173,7 +173,7 @@
     for p in range(half):
         send1[p] = part[:, PAIR * p : PAIR * (p + 1)]
 
-    pl.semaphore_wait(bar, n_tp - 1 + 2 * (n_ep - 1))
+    pl.semaphore_wait(bar, n_tp - 1 + n_ep - 1)
     for r in sorted(range(1, n_tp), key=lambda r: -min(r, n_tp - r)):
         to = lax.rem(me_tp + r, n_tp)
         pltpu.make_async_remote_copy(
@@ -210,15 +210,13 @@
     comb2 = jnp.concatenate([comb_hi.astype(f32), comb_lo.astype(f32)], axis=0).astype(bf16)
     place_t = jnp.concatenate([place, jnp.zeros((120, 128), f32)], axis=0).T.astype(bf16)
     c_dn()
-    for i in range(width // 128):
-        cols = pl.ds(128 * i, 128)
-        chunk = dcat[:, cols].astype(f32).T.astype(bf16)
-        at = 128 * i
-        while at < 128 * (i + 1):
-            t, o = at // SLOT, at % SLOT
-            n = min(SLOT - o, 128 * (i + 1) - at)
-            dnt[t, pl.ds(o, n), :] = chunk[at - 128 * i : at - 128 * i + n]
-            at += n
+    flipped = jnp.concatenate(
+        [dcat[:, pl.ds(128 * i, 128)].astype(f32).T for i in range(width // 128)], axis=0)
+    for t in range(n_tp):
+        dnt[t] = flipped[SLOT * t : SLOT * t + FOLD].astype(bf16)
+        drem[t] = jnp.concatenate(
+            [jnp.zeros((128, FOLD - 16), f32), dcat[:, SLOT * t + FOLD : SLOT * (t + 1)].astype(f32)],
+            axis=1).astype(bf16)
     mg = mgain_v[...].astype(f32).reshape(1, width)
     c_wt()
     for i in range(4):
@@ -255,6 +253,9 @@
     for v in range(n_y):
         pltpu.make_async_remote_copy(
             src_ref=dnt.at[v * 2 + 1 - c], dst_ref=dsib.at[v], send_sem=wsem.at[2], recv_sem=wsem.at[3],
+            device_id=sibling, device_id_type=MESH).start()
+        pltpu.make_async_remote_copy(
+            src_ref=drem.at[v * 2 + 1 - c], dst_ref=dsibr.at[v], send_sem=wsem.at[4], recv_sem=wsem.at[5],
             device_id=sibling, device_id_type=MESH).start()
     pltpu.make_async_copy(recv2.at[pl.ds(1, n_ep - 1)], recv2.at[pl.ds(1, n_ep - 1)], rsem.at[1]).wait()
     got = recv2[...].reshape(2 * n_ep, PAIR).astype(f32)
@@ -318,6 +319,7 @@
         more = products(dy, 1 - c)
         hid, squares = hid + more[0], squares + more[1]
     whole(dsib, wsem.at[3])
+    whole(dsibr, wsem.at[5])
     for dy in (2, n_y - 2):
         hand_copy(dy).wait_recv()
     more = products(2, 1 - c)
@@ -330,7 +332,9 @@
         ge, ue, gs, us = (hid[o + 64 * i : o + 64 * (i + 1)] for i in range(4))
         parts.append(jnp.where(routed_l, ge / (1.0 + jnp.exp(-ge)) * ue, 0.0))
         parts.append(jnp.where(routed_l, 0.0, gs / (1.0 + jnp.exp(-gs)) * us))
-    hcat = jnp.concatenate(parts, axis=0).astype(bf16)
+    hcat = jnp.concatenate(parts, axis=0)
+    hrow = hcat.T[0:FOLD].astype(bf16)
+    hcat = hcat.astype(bf16)
 
     far = (3, n_y - 3, 2, n_y - 2, 1, n_y - 1)
     far_at = {dy: i for i, dy in enumerate(far)}
@@ -343,7 +347,9 @@
             device_id={"tp": to * 2 + c}, device_id_type=MESH)
 
     def terms(v):
-        return mm(jnp.concatenate([dnt[v * 2 + c], dsib[v]], axis=1), hcat)
+        t = v * 2 + c
+        return mm(jnp.concatenate([dnt[t], dsib[v]], axis=1), hcat) + mm(
+            hrow, jnp.concatenate([drem[t], dsibr[v]], axis=0))
 
     for dy in far:
         to = lax.rem(y + dy, n_y)
@@ -355,7 +361,11 @@
     for dy in far:
         side = 0 if dy < n_y // 2 else 1
         totals[side] += recv5[far_at[dy]].astype(f32)
-    backs = [jnp.concatenate([a, jnp.zeros((LANES - SLOT, 128), f32)], axis=0).T for a in totals]
+    backs = []
+    for a in totals:
+        a = jnp.concatenate([a, jnp.zeros((128 - FOLD, 128), f32)], axis=0)
+        backs.append(jnp.concatenate(
+            [a.T[:, 0:FOLD], a[:, 128 - (SLOT - FOLD) : 128], jnp.zeros((128, LANES - SLOT), f32)], axis=1))
     shared = backs[0][2 * n_ep : 2 * n_ep + 8]
     share_s[...] = backs[1][2 * n_ep : 2 * n_ep + 8]
     for side in range(2):
@@ -376,6 +386,7 @@
     pltpu.make_async_copy(recv2.at[pl.ds(1, n_ep - 1)], recv2.at[pl.ds(1, n_ep - 1)], ssem.at[1]).wait()
     w_copy.wait_send()
     whole(dsib, wsem.at[2])
+    whole(dsibr, wsem.at[4])
     whole(xt.at[pl.ds(0, 3)], ssem.at[4])
     whole(xt.at[pl.ds(0, 4)], ssem.at[5])
     whole(recv5, ssem.at[6])
@@ -408,12 +419,13 @@
             V((1, 1), f32), pltpu.SMEM((seqs,), i32), V((width,), bf16), V((128,), bf16), V((width,), bf16),
             V(ids.shape, i32), V(ew.shape, f32),
             V((8, width), f32), V((half, 8, PAIR), f32), V((8, 128), i32), V((8, 128), f32),
-            V((n_tp, SLOT, 128), bf16), V((n_y, SLOT, 128), bf16), V((half + 1, 512, HEADK), bf16),
+            V((n_tp, FOLD, 128), bf16), V((n_tp, 128, 128), bf16),
+            V((n_y, FOLD, 128), bf16), V((n_y, 128, 128), bf16), V((half + 1, 512, HEADK), bf16),
             V((half, 8, PAIR), bf16), V((n_tp - 1, 8, PAIR), bf16),
             V((n_ep, 2, PAIR), bf16), V((n_ep, 2, PAIR), bf16),
-            V((half, BLOCK, 128), bf16), V((n_y, SLOT, 128), bf16), V((n_y - 2, SLOT, 128), bf16),
+            V((half, BLOCK, 128), bf16), V((n_y, FOLD, 128), bf16), V((n_y - 2, FOLD, 128), bf16),
             V((2, n_ep, 2, LANES), bf16), V((2, n_ep, 2, LANES), bf16), V((8, LANES), f32), V((8, LANES), f32),
-            DMA((24,)), DMA((7,)), DMA((5,)), DMA((4,)), DMA((5,)), DMA((4,)), DMA((2,)),
+            DMA((24,)), DMA((7,)), DMA((5,)), DMA((4,)), DMA((5,)), DMA((6,)), DMA((2,)),
         ]
         return pl.pallas_call(
             functools.partial(kernel, n_ep, n_tp),

time: 57.5 us -> 56.5 us (0.983)
  Pallas kernels: 56.1 us -> 55.2 us
    pallas_call x1, Pallas kernels: 56.1 us -> 55.2 us  [step(): pl.pallas_call(functools.partial(kernel, n_ep, n_tp), out_shape=pltpu.VME...]
where the time goes in v4:
time: 56.5 us; the launch traced here: 56.4 us
  Pallas kernels  55.2 us (98%)
  between operations  0.66 us (1%)
  local copies, waits for them, and re-layouts  0.6 us (1%)
    pallas_call x1, Pallas kernels, step(): pl.pallas_call(functools.partial(kernel, n_ep, n_tp), out_shape=pltpu.VME...  55.2 us

profile of v4, /device:TPU:1, one launch (start us, length us, event | category | flops | bytes accessed | tf_op | source)
XLA Modules:
  0.0 56.4 jit_solution(10400366412961067874)
XLA Ops:
  0.7 55.2 %decode_step.1 = bf16[7,144]{1,0:T(8,128)(2,1)S(1)} custom-call(bf16[7,2304]{1,0:T(8,128)(2,1)} %tok.1, bf16[2304]{0:T(1024)(128)(2,1)} %again.1, bf16[2304,128]{1,0:T(8,128)(2,1)} %wq.1, bf16[2304,128]{1,0:T(8,128)(2,1)} %wk.1, bf16[2304,128]{1,0:T(8,128)(2,1)} %wv.1, bf16[2304,128]{1,0:T(8,128)(2,1)} %ow.1, f32[1,1]{1,0:T(1,128)} %bitcast.12.lam, ...), custom_call_target="tpu_custom_call" | custom-call | tf_op jit(solution)/shard_map/decode_step/pallas_call | solution.py:430
  55.8 0.6 %copy.22 = bf16[7,144]{1,0:T(8,128)(2,1)} copy(bf16[7,144]{1,0:T(8,128)(2,1)S(1)} %decode_step.1) | data formatting | bytes 4032

commit v5 on v4

--- a/solution.py
+++ b/solution.py
@@ -40,7 +40,7 @@
     tok_v, wqkv, k_v, v_v, ow_v, wt, dcat, lam_v, lens_s, again_v, hgain_v, mgain_v, ids_v, ew_v,
     x_s, tokblk, idp, ewp, dnt, drem, dsib, dsibr, wp,
     send1, recv1, send2, recv2, xt, q5, recv5, send6, recv6, share_s, share_r,
-    lsem, ssem, rsem, r3, f3r, wsem, hsem,
+    lsem, ssem, rsem, r3, f3r, wsem, hsem, here,
 ):
     n_z, n_y = n_ep // NX, n_tp // 2
     seqs, width = tok.shape
@@ -89,16 +89,14 @@
                  dst.at[p, :, pl.ds(0, 128 * min(2, seqs - 2 * p))])
             for p in range((seqs + 1) // 2)]
 
-    for slot in slots:
-        pl.semaphore_signal(bar, inc=1, device_id={"ep": ep_at(slot)}, device_id_type=MESH)
-    for r in range(1, n_tp):
-        pl.semaphore_signal(bar, inc=1, device_id={"tp": lax.rem(me_tp + r, n_tp)}, device_id_type=MESH)
     c_tok, c_gain = load([(tok, tok_v)]), load([(again, again_v)])
     step = width // 3
     c_qkv = [
         load([(w.at[pl.ds(step * j, step)], wqkv.at[pl.ds(step * j, step), pl.ds(128 * i, 128)])
               for i, w in enumerate((wq, wk, wv))], wqkv.at[pl.ds(step * j, step)])
         for j in range(3)]
+    for r in range(1, n_tp):
+        pl.semaphore_signal(bar, inc=1, device_id={"tp": lax.rem(me_tp + r, n_tp)}, device_id_type=MESH)
     c_k = cached(ck, k_v)
     c_len, c_lam, c_hgain = load([(lens, lens_s)]), load([(lam, lam_v)]), load([(hgain, hgain_v)])
     c_v = cached(cv, v_v)
@@ -108,6 +106,13 @@
     c_ids, c_ew, c_mgain = load([(ids, ids_v)]), load([(ew, ew_v)]), load([(mgain, mgain_v)])
     c_dn = load([(w, dcat.at[pl.ds(64 * i, 64)]) for i, w in enumerate((dw, sd))], dcat)
     c_wt = load([(w, wt.at[pl.ds(64 * i, 64)]) for i, w in enumerate((gwt, uwt, sgt, sut))], wt)
+
+    for slot in slots:
+        greeted = ep_at(slot)
+
+        @pl.when(greeted > me_ep)
+        def greet():
+            pl.semaphore_signal(bar, inc=1, device_id={"ep": greeted}, device_id_type=MESH)
 
     x_s[...] = jnp.zeros_like(x_s)
     if seqs % 2:
@@ -169,16 +174,30 @@
     hg = hgain_v[...].astype(f32).reshape(1, 128)
     head_n = (head * lax.rsqrt(jnp.mean(head * head, axis=-1, keepdims=True) + EPS) * hg).astype(bf16)
     c_ow()
-    part = mm_nt(head_n, ow_v[...].reshape(half * PAIR, 128)).astype(bf16)
+    tail = ow_v[:, pl.ds(HEADK, TAILK), :]
+    for k in range(1, 8):
+        ow_v[:, pl.ds(HEADK + TAILK * k, TAILK), :] = tail
+    part = mm_nt(head_n, ow_v[...].reshape(half * 2 * HEADK, 128))
+    row_h = lax.broadcasted_iota(i32, (8, HEADK), 0)
+    in_tail = lax.broadcasted_iota(i32, (8, HEADK), 1) // TAILK == row_h
     for p in range(half):
-        send1[p] = part[:, PAIR * p : PAIR * (p + 1)]
-
-    pl.semaphore_wait(bar, n_tp - 1 + n_ep - 1)
+        o = 2 * HEADK * p
+        tails = jnp.sum(jnp.where(in_tail, part[:, o + HEADK : o + 2 * HEADK], 0.0), axis=0, keepdims=True)
+        send1[p] = jnp.where(row_h == 7, tails, part[:, o : o + HEADK]).astype(bf16)
+
+    pl.semaphore_wait(bar, n_tp - 1 + me_ep)
     for r in sorted(range(1, n_tp), key=lambda r: -min(r, n_tp - r)):
         to = lax.rem(me_tp + r, n_tp)
         pltpu.make_async_remote_copy(
             src_ref=send1.at[lax.rem(to, half)], dst_ref=recv1.at[r - 1], send_sem=ssem.at[0], recv_sem=rsem.at[0],
             device_id={"tp": to}, device_id_type=MESH).start()
+
+    for slot in slots:
+        answered = ep_at(slot)
+
+        @pl.when(answered < me_ep)
+        def answer():
+            pl.semaphore_signal(here, inc=1, device_id={"ep": answered}, device_id_type=MESH)
 
     for p in range(half):
         q0, q1 = SLOT * p, SLOT * (p + half)
@@ -232,7 +251,12 @@
     own_part = send1[pair].astype(f32)
     own_tok = tokblk[pair]
     whole(recv1, rsem.at[0])
-    attn = own_part + jnp.sum(recv1[...].astype(f32), axis=0)
+    sums = own_part + jnp.sum(recv1[...].astype(f32), axis=0)
+    tails = jnp.where(in_tail, sums[7:8, :], 0.0)
+    tails = tails[:, 0:128] + tails[:, 128:256]
+    tails = tails + pltpu.roll(tails, 64, 1)
+    tails = tails + pltpu.roll(tails, 32, 1)
+    attn = jnp.concatenate([jnp.where(row_h == 7, 0.0, sums), tails], axis=1)
     lane2 = lax.broadcasted_iota(i32, (8, PAIR), 1)
     mixed = jnp.where(lane2 < BLOCK, own_tok + attn, 0.0).astype(bf16)
     mixed_f = mixed.astype(f32)
@@ -240,6 +264,10 @@
     mixed_p = jnp.concatenate([mixed_f, jnp.zeros((120, PAIR), f32)], axis=0).astype(bf16)
     rows = mm(place_t, mixed_p)[0 : 2 * n_ep].astype(bf16)
     send2[...] = rows.reshape(n_ep, 2, PAIR)
+
+    @pl.when(me_ep < n_ep - 1)
+    def answers():
+        pl.semaphore_wait(here, n_ep - 1 - me_ep)
 
     for slot in slots:
         pltpu.make_async_remote_copy(
@@ -415,17 +443,17 @@
         V, DMA = pltpu.VMEM, pltpu.SemaphoreType.DMA
         scratch = [
             V((seqs, width), bf16), V((width, 384), bf16), V((pairs, cache, 256), bf16), V((pairs, cache, 256), bf16),
-            V((half, PAIR, 128), bf16), V((256, width), bf16), V((128, width), bf16),
+            V((half, 2 * HEADK, 128), bf16), V((256, width), bf16), V((128, width), bf16),
             V((1, 1), f32), pltpu.SMEM((seqs,), i32), V((width,), bf16), V((128,), bf16), V((width,), bf16),
             V(ids.shape, i32), V(ew.shape, f32),
             V((8, width), f32), V((half, 8, PAIR), f32), V((8, 128), i32), V((8, 128), f32),
             V((n_tp, FOLD, 128), bf16), V((n_tp, 128, 128), bf16),
             V((n_y, FOLD, 128), bf16), V((n_y, 128, 128), bf16), V((half + 1, 512, HEADK), bf16),
-            V((half, 8, PAIR), bf16), V((n_tp - 1, 8, PAIR), bf16),
+            V((half, 8, HEADK), bf16), V((n_tp - 1, 8, HEADK), bf16),
             V((n_ep, 2, PAIR), bf16), V((n_ep, 2, PAIR), bf16),
             V((half, BLOCK, 128), bf16), V((n_y, FOLD, 128), bf16), V((n_y - 2, FOLD, 128), bf16),
             V((2, n_ep, 2, LANES), bf16), V((2, n_ep, 2, LANES), bf16), V((8, LANES), f32), V((8, LANES), f32),
-            DMA((24,)), DMA((7,)), DMA((5,)), DMA((4,)), DMA((5,)), DMA((6,)), DMA((2,)),
+            DMA((24,)), DMA((7,)), DMA((5,)), DMA((4,)), DMA((5,)), DMA((6,)), DMA((2,)), pltpu.SemaphoreType.REGULAR,
         ]
         return pl.pallas_call(
             functools.partial(kernel, n_ep, n_tp),

time: 56.5 us -> 55.6 us (0.984)
  Pallas kernels: 55.2 us -> 54.2 us
    pallas_call x1, Pallas kernels: 55.2 us -> 54.2 us  [step(): pl.pallas_call(functools.partial(kernel, n_ep, n_tp), out_shape=pltpu.VME...]
where the time goes in v5:
time: 55.6 us; the launch traced here: 55.5 us
  Pallas kernels  54.2 us (97%)
  between operations  0.66 us (1%)
  local copies, waits for them, and re-layouts  0.6 us (1%)
    pallas_call x1, Pallas kernels, step(): pl.pallas_call(functools.partial(kernel, n_ep, n_tp), out_shape=pltpu.VME...  54.2 us

profile of v5, /device:TPU:1, one launch (start us, length us, event | category | flops | bytes accessed | tf_op | source)
XLA Modules:
  0.0 55.5 jit_solution(13540554135471811656)
XLA Ops:
  0.7 54.2 %decode_step.1 = bf16[7,144]{1,0:T(8,128)(2,1)S(1)} custom-call(bf16[7,2304]{1,0:T(8,128)(2,1)} %tok.1, bf16[2304]{0:T(1024)(128)(2,1)} %again.1, bf16[2304,128]{1,0:T(8,128)(2,1)} %wq.1, bf16[2304,128]{1,0:T(8,128)(2,1)} %wk.1, bf16[2304,128]{1,0:T(8,128)(2,1)} %wv.1, bf16[2304,128]{1,0:T(8,128)(2,1)} %ow.1, f32[1,1]{1,0:T(1,128)} %bitcast.12.lam, ...), custom_call_target="tpu_custom_call" | custom-call | tf_op jit(solution)/shard_map/decode_step/pallas_call | solution.py:458
  54.9 0.6 %copy.22 = bf16[7,144]{1,0:T(8,128)(2,1)} copy(bf16[7,144]{1,0:T(8,128)(2,1)S(1)} %decode_step.1) | data formatting | bytes 4032
